TPU v7x, 32 devices: a whole 2x2x4 slice. The times are simulated.
32 devices in a mesh: fs: 8 (over z, y), tp: 4 (over x, core).
Axes of the slice: x: 2, y: 2, z: 4, core: 2. Of those that a mesh axis runs over, the one named last changes fastest.
Arguments:
- tokens: bfloat16 [512, 2048], P('fs', 'tp'), may hold values from -6 to 6
- norm_gain: float32 [2048], P('fs'), may hold values from 0.1 to 1.9
- gate_weight: float32 [8, 2048, 512], P(None, 'fs', 'tp'), may hold values from -0.125 to 0.125
- up_weight: float32 [8, 2048, 512], P(None, 'fs', 'tp'), may hold values from -0.125 to 0.125
- down_weight: float32 [8, 2048, 512], P(None, 'fs', 'tp'), may hold values from -0.25 to 0.25
- route_ids: int32 [512, 2], P('fs'), may hold values from 0 to 7, all different within a row; in each aligned block of 64 rows (0 to 63, 64 to 127, ...) at most 24 rows name the same one
- group_weight: float32 [512], P('fs'), may hold values from 0.3 to 1
- logit_gap: float32 [512], P('fs'), may hold values from -6 to 6
Outputs:
- gate_new: bfloat16 [8, 2048, 512], P('fs', None, 'tp')
- up_new: bfloat16 [8, 2048, 512], P('fs', None, 'tp')
- down_new: bfloat16 [8, 2048, 512], P('fs', None, 'tp')
- mixed: bfloat16 [512, 2048], P('fs', 'tp')
Inputs may be any that keep to these rules, and one draw needn't show every extreme that they name: `route_ids`: each row names two different experts. In the rows of one device no expert is named by more than 24 rows, a bound that some block reaches.
All inputs are finite; a program needn't handle non-finite values.
Results may differ from a plain program's by a relative error of at most 0.011.
Values may be sent and summed in bfloat16 or wider, within the bound.
No kernel may reach another device: no remote copies, remote signals or barrier semaphores. Data moves between devices by JAX's collectives and lax.ppermute only.
A program may use at most 64 MiB of HBM per device.

v0:
```python
import jax
import jax.numpy as jnp
from jax import lax
from jax.sharding import PartitionSpec as P


def slot_tables(route_ids, experts, capacity):
    row_count = route_ids.shape[0]
    pair_count = 2 * row_count
    flat_ids = route_ids.reshape(pair_count)
    onehot = (flat_ids[:, None] == jnp.arange(experts, dtype=jnp.int32)[None, :]).astype(
        jnp.bfloat16
    )
    positions = jnp.arange(pair_count, dtype=jnp.int32)
    below_mask = (positions[:, None] > positions[None, :]).astype(jnp.bfloat16)
    before = jnp.dot(below_mask, onehot, preferred_element_type=jnp.float32)
    ranked = jnp.sum(before * onehot.astype(jnp.float32), axis=1).astype(jnp.int32)
    return (flat_ids * capacity + ranked).reshape(row_count, 2)


def first_products(slot_rows, gate_cols, up_cols):
    shard_cols = lax.all_gather(slot_rows, "tp", axis=1, tiled=True)
    return (
        jnp.dot(shard_cols, gate_cols, preferred_element_type=jnp.float32),
        jnp.dot(shard_cols, up_cols, preferred_element_type=jnp.float32),
    )


def body(
    tokens, norm_gain, gate_weight, up_weight, down_weight, route_ids, group_weight, logit_gap
):
    experts = gate_weight.shape[0]
    tok_rows = tokens.shape[0]
    capacity = max(2, (3 * tok_rows + experts - 1) // experts)
    folded = norm_gain[None, :, None]
    gate_local = (gate_weight * folded).astype(jnp.bfloat16)
    up_local = (up_weight * folded).astype(jnp.bfloat16)
    down_local = down_weight.astype(jnp.bfloat16)
    slot_ids = slot_tables(route_ids, experts, capacity)
    slot_range = jnp.arange(experts * capacity, dtype=jnp.int32)
    matches = (slot_ids[None, :, :] == slot_range[:, None, None]).astype(jnp.int32)
    dispatch = jnp.sum(matches, axis=2).astype(jnp.bfloat16)
    outgoing = jnp.dot(dispatch, tokens, preferred_element_type=jnp.float32).astype(jnp.bfloat16)
    outgoing = outgoing.reshape(experts, capacity, tokens.shape[1])
    arrived = lax.all_to_all(outgoing, "fs", split_axis=0, concat_axis=0, tiled=True)
    slot_rows = arrived.reshape(experts * capacity, tokens.shape[1])
    gate_out, up_out, down_out = (
        lax.all_to_all(gate_local, "fs", split_axis=0, concat_axis=1, tiled=True),
        lax.all_to_all(up_local, "fs", split_axis=0, concat_axis=1, tiled=True),
        lax.all_to_all(down_local, "fs", split_axis=0, concat_axis=1, tiled=True),
    )
    gate_acc, up_acc = first_products(slot_rows, gate_out[0], up_out[0])
    hidden = (jax.nn.silu(gate_acc) * up_acc).astype(jnp.bfloat16)
    partial_value = lax.dot_general(
        hidden, down_out[0], (((1,), (1,)), ((), ())), preferred_element_type=jnp.float32
    )
    summed = lax.psum_scatter(
        partial_value.astype(jnp.bfloat16), "tp", scatter_dimension=1, tiled=True
    )
    returned = lax.all_to_all(
        summed.reshape(experts, capacity, summed.shape[1]),
        "fs",
        split_axis=0,
        concat_axis=0,
        tiled=True,
    )
    back_rows = returned.reshape(experts * capacity, summed.shape[1])
    pick_first = (slot_ids[:, 0:1] == slot_range[None, :]).astype(jnp.bfloat16)
    pick_second = (slot_ids[:, 1:2] == slot_range[None, :]).astype(jnp.bfloat16)
    first_vals = jnp.dot(pick_first, back_rows, preferred_element_type=jnp.float32)
    second_vals = jnp.dot(pick_second, back_rows, preferred_element_type=jnp.float32)
    first_weight = group_weight * jax.nn.sigmoid(logit_gap)
    second_weight = group_weight * jax.nn.sigmoid(-logit_gap)
    mixed = (first_weight[:, None] * first_vals + second_weight[:, None] * second_vals).astype(
        jnp.bfloat16
    )
    return (gate_out, up_out, down_out, mixed)


def solution(mesh):
    return jax.shard_map(
        body,
        mesh=mesh,
        in_specs=(
            P("fs", "tp"),
            P("fs"),
            P(None, "fs", "tp"),
            P(None, "fs", "tp"),
            P(None, "fs", "tp"),
            P("fs", None),
            P("fs"),
            P("fs"),
        ),
        out_specs=(P("fs", None, "tp"), P("fs", None, "tp"), P("fs", None, "tp"), P("fs", "tp")),
        check_vma=False,
    )
```

profile of v0, /device:TPU:0, one launch (start us, length us, event | category | flops | bytes accessed | tf_op | source)
XLA Modules:
  0.0 126.2 jit_solution(10484632663236420106)
XLA Ops:
  7.2 0.0 copy-start
  7.2 0.8 copy.22
  8.0 0.1 eq.58
  8.1 0.1 fusion.3
  8.3 0.1 convert_element_type.51
  8.4 0.1 copy.23
  8.5 0.7 multiply_add_fusion
  9.2 0.1 convert_reduce_fusion
  9.3 0.0 copy-done
  9.3 0.9 convolution_convert_fusion.1
  10.2 7.3 %all-to-all-start.3 = ((bf16[8,24,512]{2,1,0:T(8,128)(2,1)}), bf16[8,24,512]{2,1,0:T(8,128)(2,1)S(1)}, u32[]{:S(2)}, u32[]{:S(2)}) async-start(bf16[8,24,512]{2,1,0:T(8,128)(2,1)} %bitcast.4), calls=%async_computation.3 | async-start | bytes 393216 | tf_op jit(solution)/shard_map/all_to_all | solution.py:45
  17.5 2.7 %multiply_convert_fusion = (bf16[8,256,128]{2,1,0:T(8,128)(2,1)}, bf16[8,256,128]{2,1,0:T(8,128)(2,1)S(1)}) fusion(f32[8,256,128]{2,1,0:T(8,128)} %param.11, f32[256]{0:T(256)} %param.9, f32[8,256,128]{2,1,0:T(8,128)} %param.10), kind=kLoop, calls=%fused_computation.10 | loop fusion | flops 1048576 | bytes 3146752 | tf_op jit(solution)/shard_map/convert_element_type | solution.py:37
  20.2 5.3 %all-to-all-done.3 = bf16[8,24,512]{2,1,0:T(8,128)(2,1)S(1)} async-done(((bf16[8,24,512]{2,1,0:T(8,128)(2,1)}), bf16[8,24,512]{2,1,0:T(8,128)(2,1)S(1)}, u32[]{:S(2)}, u32[]{:S(2)}) %all-to-all-start.3) | async-done | bytes 196640 | tf_op jit(solution)/shard_map/all_to_all | solution.py:45
  25.5 17.3 %all_to_all.46 = bf16[8,256,128]{2,1,0:T(8,128)(2,1)S(1)} all-to-all(bf16[8,256,128]{2,1,0:T(8,128)(2,1)S(1)} %get-tuple-element.9), channel_id=1, replica_groups=mesh['fs'=8,'tp'=4] {'fs'}, dimensions={0} | all-to-all | bytes 1048576 | tf_op jit(solution)/shard_map/all_to_all | solution.py:48
  42.8 3.6 %all-to-all-start.1 = ((bf16[8,256,128]{2,1,0:T(8,128)(2,1)}), bf16[8,256,128]{2,1,0:T(8,128)(2,1)S(1)}, u32[]{:S(2)}, u32[]{:S(2)}) async-start(bf16[8,256,128]{2,1,0:T(8,128)(2,1)} %get-tuple-element.8), calls=%async_computation.1 | async-start | bytes 1048576 | tf_op jit(solution)/shard_map/all_to_all | solution.py:49
  46.4 0.9 convert_element_type.47
  47.3 13.3 %all-to-all-done.1 = bf16[8,256,128]{2,1,0:T(8,128)(2,1)S(1)} async-done(((bf16[8,256,128]{2,1,0:T(8,128)(2,1)}), bf16[8,256,128]{2,1,0:T(8,128)(2,1)S(1)}, u32[]{:S(2)}, u32[]{:S(2)}) %all-to-all-start.1) | async-done | bytes 524320 | tf_op jit(solution)/shard_map/all_to_all | solution.py:49
  60.6 3.6 %all-to-all-start.2 = ((bf16[8,256,128]{2,1,0:T(8,128)(2,1)}), bf16[8,256,128]{2,1,0:T(8,128)(2,1)S(1)}, u32[]{:S(2)}, u32[]{:S(2)}) async-start(bf16[8,256,128]{2,1,0:T(8,128)(2,1)} %convert_element_type.47), calls=%async_computation.2 | async-start | bytes 1048576 | tf_op jit(solution)/shard_map/all_to_all | solution.py:50
  64.2 0.0 reduce-scatter.2.cloned.1.call-start
  64.3 8.6 %all_gather.3 = bf16[192,2048]{1,0:T(8,128)(2,1)S(1)} all-gather(bf16[192,512]{1,0:T(8,128)(2,1)S(1)} %bitcast.30), channel_id=1, replica_groups=mesh['fs'=8,'tp'=4] {'tp'}, dimensions={1}, use_global_device_ids=true | all-gather | bytes 983040 | tf_op jit(solution)/shard_map/all_gather | solution.py:22
  72.9 0.3 fusion.16
  73.2 5.4 %all-to-all-done.2 = bf16[8,256,128]{2,1,0:T(8,128)(2,1)S(1)} async-done(((bf16[8,256,128]{2,1,0:T(8,128)(2,1)}), bf16[8,256,128]{2,1,0:T(8,128)(2,1)S(1)}, u32[]{:S(2)}, u32[]{:S(2)}) %all-to-all-start.2) | async-done | bytes 524320 | tf_op jit(solution)/shard_map/all_to_all | solution.py:50
  78.7 1.5 %convolution_convert_fusion = bf16[192,2048]{1,0:T(8,128)(2,1)} fusion(bf16[2048,128]{1,0:T(8,128)(2,1)S(1)} %bitcast.26, bf16[192,2048]{1,0:T(8,128)(2,1)S(1)} %all_gather.3, bf16[2048,128]{1,0:T(8,128)(2,1)S(1)} %bitcast.24, f32[192,128]{1,0:T(8,128)S(1)} %fusion.16), kind=kOutput, calls=%fused_computation | convolution fusion | flops 201867264 | bytes 2719744 | tf_op jit(solution)/shard_map/dot_general | solution.py:54
  80.2 0.0 reduce-scatter.2.cloned.1.call-update
  80.2 22.4 %reduce-scatter.2.cloned.1.call-done = bf16[192,512]{1,0:T(8,128)(2,1)} async-done(((bf16[192,2048]{1,0:T(8,128)(2,1)}), bf16[192,512]{1,0:T(8,128)(2,1)}) %reduce-scatter.2.cloned.1.call-update) | async-done | bytes 196624 | tf_op jit(solution)/shard_map/reduce_scatter | solution.py:57
  102.6 5.5 %all-to-all-start.4 = ((bf16[8,24,512]{2,1,0:T(8,128)(2,1)}), bf16[8,24,512]{2,1,0:T(8,128)(2,1)S(1)}, u32[]{:S(2)}, u32[]{:S(2)}) async-start(bf16[8,24,512]{2,1,0:T(8,128)(2,1)} %bitcast.31), calls=%async_computation.5 | async-start | bytes 393216 | tf_op jit(solution)/shard_map/all_to_all | solution.py:60
  108.2 7.8 %all-to-all-done.4 = bf16[8,24,512]{2,1,0:T(8,128)(2,1)S(1)} async-done(((bf16[8,24,512]{2,1,0:T(8,128)(2,1)}), bf16[8,24,512]{2,1,0:T(8,128)(2,1)S(1)}, u32[]{:S(2)}, u32[]{:S(2)}) %all-to-all-start.4) | async-done | bytes 196640 | tf_op jit(solution)/shard_map/all_to_all | solution.py:60
  116.0 0.2 convolution_multiply_fusion
  116.2 0.8 fusion.1
  117.0 0.8 copy.27
  117.8 0.8 copy.28
  118.6 0.8 copy.29
  (9 shorter events, 0.0 us)
Async XLA Ops:
  7.2 2.1 %copy-start = (bf16[64,512]{1,0:T(8,128)(2,1)S(1)}, bf16[64,512]{1,0:T(8,128)(2,1)}, u32[]{:S(2)}) copy-start(bf16[64,512]{1,0:T(8,128)(2,1)} %param.8) | copy-start | bytes 196612
  10.2 15.3 %all-to-all-start.3 = ((bf16[8,24,512]{2,1,0:T(8,128)(2,1)}), bf16[8,24,512]{2,1,0:T(8,128)(2,1)S(1)}, u32[]{:S(2)}, u32[]{:S(2)}) async-start(bf16[8,24,512]{2,1,0:T(8,128)(2,1)} %bitcast.4), calls=%async_computation.3 | async-start | bytes 393216 | tf_op jit(solution)/shard_map/all_to_all | solution.py:45
  25.5 20.9 %copy-start.1 = (f32[8,256,128]{2,1,0:T(8,128)S(1)}, f32[8,256,128]{2,1,0:T(8,128)}, u32[]{:S(2)}) copy-start(f32[8,256,128]{2,1,0:T(8,128)} %param.12) | copy-start | bytes 3145732
  42.8 17.8 %all-to-all-start.1 = ((bf16[8,256,128]{2,1,0:T(8,128)(2,1)}), bf16[8,256,128]{2,1,0:T(8,128)(2,1)S(1)}, u32[]{:S(2)}, u32[]{:S(2)}) async-start(bf16[8,256,128]{2,1,0:T(8,128)(2,1)} %get-tuple-element.8), calls=%async_computation.1 | async-start | bytes 1048576 | tf_op jit(solution)/shard_map/all_to_all | solution.py:49
  60.6 18.1 %all-to-all-start.2 = ((bf16[8,256,128]{2,1,0:T(8,128)(2,1)}), bf16[8,256,128]{2,1,0:T(8,128)(2,1)S(1)}, u32[]{:S(2)}, u32[]{:S(2)}) async-start(bf16[8,256,128]{2,1,0:T(8,128)(2,1)} %convert_element_type.47), calls=%async_computation.2 | async-start | bytes 1048576 | tf_op jit(solution)/shard_map/all_to_all | solution.py:50
  64.2 38.4 %reduce-scatter.2.cloned.1.call-start = ((), (), s32[]{:S(2)}) async-start(), calls=%async_computation.6 | async-start | bytes 983040 | tf_op jit(solution)/shard_map/reduce_scatter | solution.py:57
  80.2 28.0 %copy-start.2 = (f32[64]{0:T(128)S(1)}, f32[64]{0:T(128)}, u32[]{:S(2)}) copy-start(f32[64]{0:T(128)} %param.14) | copy-start | bytes 772
  80.2 28.0 %copy-start.3 = (f32[64]{0:T(128)S(1)}, f32[64]{0:T(128)}, u32[]{:S(2)}) copy-start(f32[64]{0:T(128)} %param.15) | copy-start | bytes 772
  102.6 13.3 %all-to-all-start.4 = ((bf16[8,24,512]{2,1,0:T(8,128)(2,1)}), bf16[8,24,512]{2,1,0:T(8,128)(2,1)S(1)}, u32[]{:S(2)}, u32[]{:S(2)}) async-start(bf16[8,24,512]{2,1,0:T(8,128)(2,1)} %bitcast.31), calls=%async_computation.5 | async-start | bytes 393216 | tf_op jit(solution)/shard_map/all_to_all | solution.py:60
Sparse Core Ops, SparseCore 0:
  80.4 22.2 reduce-scatter.1
where the time goes:
time: 127 us; the launch traced here: 126 us
  waiting for transfers between devices  54.2 us (43%)
  blocking collectives  25.9 us (20%)
  starting transfers between devices  20.1 us (16%)
  between operations  14.1 us (11%)
  other arithmetic  4.34 us (3%)
  matrix products  4 us (3%)
  local copies, waits for them, and re-layouts  3.56 us (3%)
    reduce_scatter x1, waiting for transfers between devices, body(): lax.psum_scatter(partial_value.astype(jnp.bfloat16), 'tp', scatter_dimens...  22.4 us
    all_to_all x1, blocking collectives, body(): lax.all_to_all(gate_local, 'fs', split_axis=0, concat_axis=1, tiled=True)  17.3 us
    all_to_all x1, waiting for transfers between devices, body(): lax.all_to_all(up_local, 'fs', split_axis=0, concat_axis=1, tiled=True)  13.3 us
    all_gather x1, blocking collectives, first_products(): shard_cols = lax.all_gather(slot_rows, 'tp', axis=1, tiled=True)  8.6 us
    all_to_all x1, waiting for transfers between devices, body(): lax.all_to_all(summed.reshape(experts, capacity, summed.shape[1]), 'fs',...  7.75 us
    all_to_all x1, starting transfers between devices, body(): lax.all_to_all(outgoing, 'fs', split_axis=0, concat_axis=0, tiled=True)  7.31 us
    all_to_all x1, starting transfers between devices, body(): lax.all_to_all(summed.reshape(experts, capacity, summed.shape[1]), 'fs',...  5.51 us
    all_to_all x1, waiting for transfers between devices, body(): lax.all_to_all(down_local, 'fs', split_axis=0, concat_axis=1, tiled=True)  5.44 us
  transfers between devices with their start and end apart: 5, of which 5 were waited for; matrix products, arithmetic and copies ran while one was open for 3% of the time, Pallas kernels for 0%

commit v1 on v0

--- a/solution.py
+++ b/solution.py
@@ -1,7 +1,520 @@
 import jax
 import jax.numpy as jnp
 from jax import lax
+from jax.experimental import pallas as pl
+from jax.experimental.pallas import tpu as pltpu
 from jax.sharding import PartitionSpec as P
+
+
+BF16 = jnp.bfloat16
+F32 = jnp.float32
+
+
+GRANT = pltpu.CompilerParams(vmem_limit_bytes=8 * 1024 * 1024)
+VMEM = pltpu.VMEM
+ANY = pl.ANY
+
+
+def whole(space):
+    return pl.BlockSpec(memory_space=space)
+
+
+def column(row):
+    n = row.shape[1]
+    same = lax.broadcasted_iota(jnp.int32, (n, n), 0) == lax.broadcasted_iota(jnp.int32, (n, n), 1)
+    return jnp.sum(jnp.where(same, row, 0.0), axis=1, keepdims=True)
+
+
+def own_places():
+    return lax.axis_index("fs").astype(jnp.int32), lax.axis_index("tp").astype(jnp.int32)
+
+
+def put_rows(target, base, rows):
+    capacity, features = rows.shape
+    cols = target.shape[1]
+    for c in range(features // cols):
+        at = base + c * capacity
+        target[at : at + capacity, :] = rows[:, c * cols : (c + 1) * cols]
+
+
+def fetch(pairs, sems):
+    copies = []
+    for n, (source, target) in enumerate(pairs):
+        copy = pltpu.make_async_copy(source, target, sems.at[n])
+        copy.start()
+        copies.append(copy)
+    return copies
+
+
+def start_first(
+    steps, later, routes, group_weight, logit_gap, tokens, gain, weights, capacity, ratio
+):
+    tok_rows, features = tokens.shape
+    experts, block, cols = weights[0].shape
+    stack, count = len(weights), len(steps)
+    lanes = features // cols
+    height = stack * block + lanes * capacity
+    small = (routes, group_weight, logit_gap, tokens, gain)
+
+    def kernel(*refs):
+        small_in = refs[: len(small)]
+        sources = refs[len(small) : len(small) + stack]
+        at = len(small) + stack
+        info_ref, later_ref = refs[at : at + 2]
+        targets = refs[at + 2 : at + 2 + count]
+        small_refs = refs[at + 2 + count : at + 2 + count + len(small)]
+        buffer, small_sems, sems = refs[at + 2 + count + len(small) :]
+        route_ref, group_ref, gap_ref, tok_ref, gain_ref = small_refs
+        own, _ = own_places()
+        small_copies = fetch(list(zip(small_in, small_refs)), small_sems)
+        order = [(n, w) for n in range(count) for w in range(stack)]
+        copies = fetch(
+            [(sources[w].at[own ^ steps[n]], buffer.at[n, w]) for n, w in order], sems
+        )
+        for copy in small_copies:
+            copy.wait()
+        first = route_ref[0:1, :]
+        second = route_ref[1:2, :]
+        names = lax.broadcasted_iota(jnp.int32, (experts, tok_rows), 0)
+        hit_first = (names == first).astype(F32)
+        hit_second = (names == second).astype(F32)
+        shape = (tok_rows, tok_rows)
+        above = lax.broadcasted_iota(jnp.int32, shape, 0) < lax.broadcasted_iota(jnp.int32, shape, 1)
+        before = jnp.dot(
+            (hit_first + hit_second).astype(BF16),
+            above.astype(F32).astype(BF16),
+            preferred_element_type=F32,
+        )
+        rank_first = jnp.sum(before * hit_first, axis=0, keepdims=True).astype(jnp.int32)
+        rank_second = jnp.sum(before * hit_second, axis=0, keepdims=True).astype(jnp.int32)
+        slots = lax.broadcasted_iota(jnp.int32, (experts * capacity, tok_rows), 0)
+        there_first = (first ^ own) * capacity + rank_first
+        there_second = (second ^ own) * capacity + rank_second
+        chosen = ((there_first == slots) | (there_second == slots)).astype(F32).astype(BF16)
+        outgoing = jnp.dot(chosen, tok_ref[...], preferred_element_type=F32).astype(BF16)
+        for n, s in enumerate(steps):
+            put_rows(targets[n], stack * block, outgoing[s * capacity : (s + 1) * capacity])
+        for n, s in enumerate(later):
+            put_rows(later_ref.at[n], 0, outgoing[s * capacity : (s + 1) * capacity])
+        gap = gap_ref[...]
+        group = group_ref[...]
+        info_ref[:, 0:1] = column(group * jax.nn.sigmoid(gap))
+        info_ref[:, 1:2] = column(group * jax.nn.sigmoid(-gap))
+        for k in range(ratio):
+            for c, (name, rank) in enumerate(((first, rank_first), (second, rank_second))):
+                place = (name // ratio) * capacity + rank
+                place = jnp.where(name % ratio == k, place, -1)
+                info_ref[:, 2 + 2 * k + c : 3 + 2 * k + c] = column(place.astype(F32))
+        factor = column(gain_ref[...])
+        for (n, w), copy in zip(order, copies):
+            copy.wait()
+            targets[n][w * block : (w + 1) * block, :] = (buffer[n, w] * factor).astype(BF16)
+
+    return pl.pallas_call(
+        kernel,
+        in_specs=[whole(ANY)] * (len(small) + stack),
+        out_specs=[whole(VMEM)] * (2 + count),
+        out_shape=[
+            jax.ShapeDtypeStruct((tok_rows, 2 + 2 * ratio), F32),
+            jax.ShapeDtypeStruct((len(later), lanes * capacity, cols), BF16),
+        ]
+        + [jax.ShapeDtypeStruct((height, cols), BF16)] * count,
+        scratch_shapes=[VMEM(value.shape, value.dtype) for value in small]
+        + [
+            VMEM((count, stack, block, cols), F32),
+            pltpu.SemaphoreType.DMA((len(small),)),
+            pltpu.SemaphoreType.DMA((count * stack,)),
+        ],
+        compiler_params=GRANT,
+        name="start_first",
+    )(*small, *weights)
+
+
+def start_later(steps, later_rows, gain, weights):
+    stack, count = len(weights), len(steps)
+    block, cols = weights[0].shape[1:]
+    tail = later_rows.shape[1]
+
+    def kernel(rows_ref, gain_ref, *refs):
+        sources = refs[:stack]
+        targets = refs[stack : stack + count]
+        buffer, sems = refs[stack + count :]
+        own, _ = own_places()
+        order = [(n, w) for n in range(count) for w in range(stack)]
+        copies = fetch(
+            [(sources[w].at[own ^ steps[n]], buffer.at[n, w]) for n, w in order], sems
+        )
+        factor = column(gain_ref[...])
+        for n in range(count):
+            targets[n][stack * block :, :] = rows_ref[n]
+        for (n, w), copy in zip(order, copies):
+            copy.wait()
+            targets[n][w * block : (w + 1) * block, :] = (buffer[n, w] * factor).astype(BF16)
+
+    return pl.pallas_call(
+        kernel,
+        in_specs=[whole(VMEM)] * 2 + [whole(ANY)] * stack,
+        out_specs=[whole(VMEM)] * count,
+        out_shape=[jax.ShapeDtypeStruct((stack * block + tail, cols), BF16)] * count,
+        scratch_shapes=[
+            VMEM((count, stack, block, cols), F32),
+            pltpu.SemaphoreType.DMA((count * stack,)),
+        ],
+        compiler_params=GRANT,
+        name="start_later",
+    )(later_rows, gain, *weights)
+
+
+def slot_rows_of(chunks, base, capacity):
+    count = len(chunks)
+    height, cols = chunks[0].shape
+    lanes = (height - base) // capacity
+
+    def kernel(*refs):
+        out = refs[count]
+        for n in range(count):
+            for c in range(lanes):
+                at = base + c * capacity
+                out[n * capacity : (n + 1) * capacity, c * cols : (c + 1) * cols] = refs[n][
+                    at : at + capacity, :
+                ]
+
+    return pl.pallas_call(
+        kernel,
+        in_specs=[whole(VMEM)] * count,
+        out_specs=whole(VMEM),
+        out_shape=jax.ShapeDtypeStruct((count * capacity, lanes * cols), BF16),
+        compiler_params=GRANT,
+        name="slot_rows",
+    )(*chunks)
+
+
+def cast_rows(weight, n_tp):
+    experts, rows, cols = weight.shape
+    part = rows // n_tp
+
+    def kernel(source, *refs):
+        targets = refs[:n_tp]
+        buffer, sems = refs[n_tp:]
+        own, lane = own_places()
+        copies = fetch([(source.at[own ^ s], buffer.at[s]) for s in range(experts)], sems)
+        for s, copy in enumerate(copies):
+            copy.wait()
+            for t in range(n_tp):
+                start = pl.multiple_of((lane ^ t) * part, part)
+                targets[t][s] = buffer[s, pl.ds(start, part), :].astype(BF16)
+
+    return pl.pallas_call(
+        kernel,
+        in_specs=[whole(ANY)],
+        out_specs=[whole(VMEM)] * n_tp,
+        out_shape=[jax.ShapeDtypeStruct((experts, part, cols), BF16)] * n_tp,
+        scratch_shapes=[
+            VMEM((experts, rows, cols), F32),
+            pltpu.SemaphoreType.DMA((experts,)),
+        ],
+        compiler_params=GRANT,
+        name="cast_rows",
+    )(weight)
+
+
+def regroup(parts):
+    inner, outer = len(parts), parts[0].shape[0]
+
+    def kernel(*refs):
+        for s in range(outer):
+            for t in range(inner):
+                refs[inner + s][t] = refs[t][s]
+
+    return pl.pallas_call(
+        kernel,
+        in_specs=[whole(VMEM)] * inner,
+        out_specs=[whole(VMEM)] * outer,
+        out_shape=[jax.ShapeDtypeStruct((inner,) + parts[0].shape[1:], parts[0].dtype)] * outer,
+        compiler_params=GRANT,
+        name="regroup",
+    )(*parts)
+
+
+def gate_up(parts, chunks, block):
+    n_fs, n_tp = len(chunks), len(parts[0])
+    ratio = n_fs // n_tp
+    cols = chunks[0].shape[1]
+    counts = [batch[0].shape[0] for batch in parts]
+    slots = sum(counts)
+    flat = [piece for batch in parts for piece in batch]
+
+    def kernel(*refs):
+        piece_refs = refs[: len(flat)]
+        chunk_refs = refs[len(flat) : len(flat) + n_fs]
+        hidden_ref, rows_ref = refs[len(flat) + n_fs :]
+        own, lane = own_places()
+        at = 0
+        for k, count in enumerate(counts):
+            for t in range(n_tp):
+                for h in range(ratio):
+                    rows_ref[(lane ^ t) * ratio + h, at : at + count] = piece_refs[k * n_tp + t][
+                        :, h * block : (h + 1) * block
+                    ]
+            at += count
+        gate_acc = jnp.zeros((slots, cols), F32)
+        up_acc = jnp.zeros((slots, cols), F32)
+        for s in range(n_fs):
+            rows = rows_ref[own ^ s]
+            gate_acc += jnp.dot(rows, chunk_refs[s][:block], preferred_element_type=F32)
+            up_acc += jnp.dot(rows, chunk_refs[s][block : 2 * block], preferred_element_type=F32)
+        hidden_ref[...] = (gate_acc / (1.0 + jnp.exp(-gate_acc)) * up_acc).astype(BF16)
+
+    return pl.pallas_call(
+        kernel,
+        in_specs=[whole(VMEM)] * (len(flat) + n_fs),
+        out_specs=whole(VMEM),
+        out_shape=jax.ShapeDtypeStruct((slots, cols), BF16),
+        scratch_shapes=[VMEM((n_fs, slots, block), BF16)],
+        compiler_params=GRANT,
+        name="gate_up",
+    )(*flat, *chunks)
+
+
+def gather_blocks(batch, pieces, own, lane, block_ref, down_ref, sems):
+    n_tp = len(pieces)
+    part = pieces[0].shape[1]
+    block = n_tp * part
+    copies = []
+    for n, s in enumerate(batch):
+        for t in range(n_tp):
+            at = pl.multiple_of((lane ^ t) * part, part)
+            block_ref[n, pl.ds(at, part), :] = pieces[t][n]
+        start = pl.multiple_of((own ^ s) * block, block)
+        copy = pltpu.make_async_copy(
+            block_ref.at[n], down_ref.at[0, pl.ds(start, block)], sems.at[n]
+        )
+        copy.start()
+        copies.append(copy)
+    return copies
+
+
+def store(chunks, block, batch, pieces):
+    n_fs, n_tp = len(chunks), len(pieces)
+    cols = chunks[0].shape[1]
+
+    def kernel(*refs):
+        piece_refs = refs[n_fs : n_fs + n_tp]
+        outs = refs[n_fs + n_tp : n_fs + n_tp + 3]
+        block_ref, sems, down_sems = refs[n_fs + n_tp + 3 :]
+        own, lane = own_places()
+        copies = gather_blocks(batch, piece_refs, own, lane, block_ref, outs[2], down_sems)
+        for s in range(n_fs):
+            start = pl.multiple_of((own ^ s) * block, block)
+            for w in range(2):
+                copy = pltpu.make_async_copy(
+                    refs[s].at[pl.ds(w * block, block)],
+                    outs[w].at[0, pl.ds(start, block)],
+                    sems.at[s, w],
+                )
+                copy.start()
+                copies.append(copy)
+        for copy in copies:
+            copy.wait()
+
+    full = jax.ShapeDtypeStruct((1, n_fs * block, cols), BF16)
+    return pl.pallas_call(
+        kernel,
+        in_specs=[whole(VMEM)] * (n_fs + n_tp),
+        out_specs=[whole(ANY)] * 3,
+        out_shape=[full] * 3,
+        scratch_shapes=[
+            VMEM((len(batch), block, cols), BF16),
+            pltpu.SemaphoreType.DMA((n_fs, 2)),
+            pltpu.SemaphoreType.DMA((len(batch),)),
+        ],
+        compiler_params=GRANT,
+        name="store",
+    )(*chunks, *pieces)
+
+
+def down(row_order, hiddens, chunks, capacity):
+    n_tp, n_fs = len(hiddens), len(chunks)
+    ratio = n_fs // n_tp
+    slots, cols = hiddens[0].shape
+    part = chunks[0].shape[1]
+
+    def kernel(*refs):
+        hidden_refs = refs[:n_tp]
+        chunk_refs = refs[n_tp : n_tp + n_fs]
+        out_ref, hidden_ref, all_ref = refs[n_tp + n_fs :]
+        own, _ = own_places()
+        for t in range(n_tp):
+            hidden_ref[:, t * cols : (t + 1) * cols] = hidden_refs[t][...]
+            for s in range(n_fs):
+                all_ref[s * part : (s + 1) * part, t * cols : (t + 1) * cols] = chunk_refs[s][t]
+        total = lax.dot_general(
+            hidden_ref[...], all_ref[...], (((1,), (1,)), ((), ())), preferred_element_type=F32
+        )
+        wide = ratio * part
+        for m in range(n_tp):
+            for k, s in enumerate(row_order):
+                out_ref[(own ^ s) * n_tp + ((own // ratio) ^ m)] = total[
+                    k * capacity : (k + 1) * capacity, m * wide : (m + 1) * wide
+                ].astype(BF16)
+
+    return pl.pallas_call(
+        kernel,
+        in_specs=[whole(VMEM)] * (n_tp + n_fs),
+        out_specs=whole(VMEM),
+        out_shape=jax.ShapeDtypeStruct((n_fs * n_tp, capacity, ratio * part), BF16),
+        scratch_shapes=[
+            VMEM((slots, n_tp * cols), BF16),
+            VMEM((n_fs * part, n_tp * cols), BF16),
+        ],
+        compiler_params=GRANT,
+        name="down",
+    )(*hiddens, *chunks)
+
+
+def finish(info, back, n_fs, batch, pieces, down_half):
+    n_tp = len(pieces)
+    part, cols = pieces[0].shape[1:]
+    capacity, wide = back.shape[1:]
+    ratio = wide // part
+    rows = info.shape[0]
+    group = n_fs // ratio
+
+    def kernel(info_ref, back_ref, *refs):
+        piece_refs = refs[:n_tp]
+        out, down_ref, block_ref, back_rows, sems = refs[n_tp + 1 :]
+        own, lane = own_places()
+        copies = gather_blocks(batch, piece_refs, own, lane, block_ref, down_ref, sems)
+        for e in range(n_fs):
+            at = (e // ratio) * capacity
+            for j in range(n_tp):
+                back_rows[e % ratio, at : at + capacity, j * wide : (j + 1) * wide] = back_ref[
+                    e * n_tp + j
+                ]
+        values = info_ref[...]
+        places = lax.broadcasted_iota(jnp.int32, (2 * rows, group * capacity), 1).astype(F32)
+        halves = []
+        for k in range(ratio):
+            both = jnp.concatenate(
+                [values[:, 2 + 2 * k : 3 + 2 * k], values[:, 3 + 2 * k : 4 + 2 * k]], axis=0
+            )
+            pick = (both == places).astype(F32).astype(BF16)
+            halves.append(jnp.dot(pick, back_rows[k], preferred_element_type=F32))
+        for y in range(ratio):
+            for j in range(n_tp):
+                total = sum(
+                    halves[k][:, j * wide + (y ^ k) * part : j * wide + ((y ^ k) + 1) * part]
+                    for k in range(ratio)
+                )
+                value = values[:, 0:1] * total[:rows] + values[:, 1:2] * total[rows:]
+                at = (y * n_tp + j) * part
+                out[:, at : at + part] = value.astype(BF16)
+        for copy in copies:
+            copy.wait()
+
+    return pl.pallas_call(
+        kernel,
+        in_specs=[whole(VMEM)] * (2 + n_tp) + [whole(ANY)],
+        out_specs=[whole(VMEM), whole(ANY)],
+        out_shape=[
+            jax.ShapeDtypeStruct((rows, n_tp * wide), BF16),
+            jax.ShapeDtypeStruct(down_half.shape, BF16),
+        ],
+        scratch_shapes=[
+            VMEM((len(batch), n_tp * part, cols), BF16),
+            VMEM((ratio, group * capacity, n_tp * wide), BF16),
+            pltpu.SemaphoreType.DMA((len(batch),)),
+        ],
+        input_output_aliases={2 + n_tp: 1},
+        compiler_params=GRANT,
+        name="finish",
+    )(info, back, *pieces, down_half)
+
+
+def exchange_body(
+    n_fs,
+    n_tp,
+    tokens,
+    norm_gain,
+    gate_weight,
+    up_weight,
+    down_weight,
+    route_ids,
+    group_weight,
+    logit_gap,
+):
+    experts = gate_weight.shape[0]
+    tok_rows = tokens.shape[0]
+    capacity = max(2, (3 * tok_rows + experts - 1) // experts)
+    block = gate_weight.shape[1]
+    far, near = halves_of(n_fs)
+    early = far[: n_fs // 4]
+    later = far[n_fs // 4 :] + near
+    batches = [near + early, far[n_fs // 4 :]]
+    row_order = batches[0] + batches[1]
+
+    def swap_fs(value, s):
+        if s == 0:
+            return value
+        return lax.ppermute(value, "fs", [(n, n ^ s) for n in range(n_fs)])
+
+    def swap_tp(value, s):
+        if s == 0:
+            return value
+        return lax.ppermute(value, "tp", [(n, n ^ s) for n in range(n_tp)])
+
+    gain = norm_gain[None, :]
+    gate_weight, up_weight, down_weight = (
+        pltpu.with_memory_space_constraint(value, pltpu.HBM)
+        for value in (gate_weight, up_weight, down_weight)
+    )
+    weights = (gate_weight, up_weight)
+    info, later_rows, *early_chunks = start_first(
+        early,
+        later,
+        *(
+            pltpu.with_memory_space_constraint(value, pltpu.HBM)
+            for value in (
+                route_ids.T,
+                group_weight[None, :],
+                logit_gap[None, :],
+                tokens,
+                gain,
+            )
+        ),
+        weights,
+        capacity,
+        n_fs // n_tp,
+    )
+    later_chunks = start_later(later, later_rows, gain, weights)
+    local = dict(zip(early + later, list(early_chunks) + list(later_chunks)))
+    chunks = [swap_fs(local[s], s) for s in range(n_fs)]
+
+    down_parts = cast_rows(down_weight, n_tp)
+    down_parts = [swap_tp(down_parts[t], t) for t in range(n_tp)]
+    down_local = regroup(down_parts)
+    down_chunks = [swap_fs(down_local[s], s) for s in range(n_fs)]
+
+    parts, quarters = [], []
+    for batch in batches:
+        rows = slot_rows_of([chunks[s] for s in batch], 2 * block, capacity)
+        parts.append([swap_tp(rows, t) for t in range(n_tp)])
+    for batch in (near, far):
+        pieces = regroup([down_chunks[s] for s in batch])
+        quarters.append([swap_tp(pieces[t], t) for t in range(n_tp)])
+
+    hidden = gate_up(parts, chunks, block)
+    hiddens = [swap_tp(hidden, t) for t in range(n_tp)]
+    rows = down(row_order, hiddens, down_chunks, capacity)
+    back = lax.all_to_all(rows, ("fs", "tp"), split_axis=0, concat_axis=0, tiled=True)
+    gate_out, up_out, down_half = store(chunks, block, near, quarters[0])
+    mixed, down_out = finish(info, back, n_fs, far, quarters[1], down_half)
+    return gate_out, up_out, down_out, mixed
+
+
+def halves_of(n_fs):
+    steps = [s ^ (n_fs - 1) for s in range(n_fs)]
+    return steps[: n_fs // 2], steps[n_fs // 2 :]
 
 
 def slot_tables(route_ids, experts, capacity):
@@ -78,8 +591,16 @@
 
 
 def solution(mesh):
+    n_fs, n_tp = mesh.shape["fs"], mesh.shape["tp"]
+    small = n_fs <= 16 and n_fs % n_tp == 0 and n_fs & (n_fs - 1) == 0
+
+    def step(*args):
+        if not small:
+            return body(*args)
+        return exchange_body(n_fs, n_tp, *args)
+
     return jax.shard_map(
-        body,
+        step,
         mesh=mesh,
         in_specs=(
             P("fs", "tp"),

time: 127 us -> 76.8 us (0.60)
  waiting for transfers between devices: 54.2 us -> 18.1 us
  starting transfers between devices: 20.1 us -> 48.4 us
  blocking collectives: 25.9 us -> 0 us
  between operations: 14.1 us -> 0.82 us
  Pallas kernels: 0 us -> 9.14 us
  other arithmetic: 4.34 us -> 0 us
  matrix products: 4 us -> 0 us
  local copies, waits for them, and re-layouts: 3.56 us -> 0.01 us
    ppermute x0 -> x32, starting transfers between devices: none -> 44.7 us  [the longest x14 32.4 us: swap_fs(): return lax.ppermute(value, 'fs', [(n, n ^ s) for n in range(n_fs)])]
    all_to_all x4 -> x1, waiting for transfers between devices: 31.8 us -> 0.01 us  [exchange_body(): lax.all_to_all(rows, ('fs', 'tp'), split_axis=0, concat_axis=0, tiled=True)]
    reduce_scatter x1 -> x0, waiting for transfers between devices: 22.4 us -> none  [body(): lax.psum_scatter(partial_value.astype(jnp.bfloat16), 'tp', scatter_dimens...]
    ppermute x0 -> x32, waiting for transfers between devices: none -> 18.1 us  [the longest x14 9.57 us: swap_fs(): return lax.ppermute(value, 'fs', [(n, n ^ s) for n in range(n_fs)])]
    all_to_all x1 -> x0, blocking collectives: 17.3 us -> none  [body(): lax.all_to_all(gate_local, 'fs', split_axis=0, concat_axis=1, tiled=True)]
    all_to_all x4 -> x1, starting transfers between devices: 20.1 us -> 3.7 us  [exchange_body(): lax.all_to_all(rows, ('fs', 'tp'), split_axis=0, concat_axis=0, tiled=True)]
    pallas_call x0 -> x12, Pallas kernels: none -> 9.14 us  [the longest x1 1.78 us: finish(): pl.pallas_call(kernel, in_specs=[whole(VMEM)] * (2 + n_tp) + [whole(ANY)]...]
    all_gather x1 -> x0, blocking collectives: 8.6 us -> none  [first_products(): shard_cols = lax.all_gather(slot_rows, 'tp', axis=1, tiled=True)]
  transfers between devices with their start and end apart: 5 -> 33, of which waited for: 5 -> 10; matrix products, arithmetic and copies ran while one was open for 3% -> 0% of each run, Pallas kernels for 0% -> 6%
where the time goes in v1:
time: 76.8 us; the launch traced here: 76.5 us
  starting transfers between devices  48.4 us (63%)
  waiting for transfers between devices  18.1 us (24%)
  Pallas kernels  9.14 us (12%)
  between operations  0.82 us (1%)
    ppermute x14, starting transfers between devices, swap_fs(): return lax.ppermute(value, 'fs', [(n, n ^ s) for n in range(n_fs)])  32.4 us
    ppermute x18, starting transfers between devices, swap_tp(): return lax.ppermute(value, 'tp', [(n, n ^ s) for n in range(n_tp)])  12.3 us
    ppermute x14, waiting for transfers between devices, swap_fs(): return lax.ppermute(value, 'fs', [(n, n ^ s) for n in range(n_fs)])  9.57 us
    ppermute x18, waiting for transfers between devices, swap_tp(): return lax.ppermute(value, 'tp', [(n, n ^ s) for n in range(n_tp)])  8.57 us
    all_to_all x1, starting transfers between devices, exchange_body(): lax.all_to_all(rows, ('fs', 'tp'), split_axis=0, concat_axis=0, tiled=True)  3.7 us
    pallas_call x1, Pallas kernels, finish(): pl.pallas_call(kernel, in_specs=[whole(VMEM)] * (2 + n_tp) + [whole(ANY)]...  1.78 us
    pallas_call x1, Pallas kernels, start_later(): pl.pallas_call(kernel, in_specs=[whole(VMEM)] * 2 + [whole(ANY)] * stack,...  1.56 us
  transfers between devices with their start and end apart: 33, of which 10 were waited for; matrix products, arithmetic and copies ran while one was open for 0% of the time, Pallas kernels for 6%

profile of v1, /device:TPU:0, one launch (start us, length us, event | category | flops | bytes accessed | tf_op | source)
XLA Modules:
  0.0 76.5 jit_solution(931431177211750666)
XLA Ops:
  0.6 1.4 %cast_rows.1 = (bf16[8,64,128]{2,1,0:T(8,128)(2,1)S(1)}, bf16[8,64,128]{2,1,0:T(8,128)(2,1)S(1)}, bf16[8,64,128]{2,1,0:T(8,128)(2,1)S(1)}, bf16[8,64,128]{2,1,0:T(8,128)(2,1)S(1)}) custom-call(f32[8,256,128]{2,1,0:T(8,128)} %source.1), custom_call_target="tpu_custom_call" | custom-call | tf_op jit(solution)/shard_map/cast_rows/pallas_call | solution.py:207
  2.6 2.6 %collective-permute-start.8 = (bf16[8,64,128]{2,1,0:T(8,128)(2,1)S(1)}, bf16[8,64,128]{2,1,0:T(8,128)(2,1)S(1)}, u32[]{:S(2)}, u32[]{:S(2)}) collective-permute-start(bf16[8,64,128]{2,1,0:T(8,128)(2,1)S(1)} %get-tuple-element.50), channel_id=1, source_target_pairs={{0,2},{1,3},{2,0},{3,1},{4,6},{5,7},{6,4},{7,5},{8,10},{9,11},{10,... | collective-permute-start | bytes 393224 | tf_op jit(solution)/shard_map/ppermute | solution.py:464
  5.2 1.4 %start_first.1 = (f32[64,6]{1,0:T(8,128)S(1)}, bf16[6,96,128]{2,1,0:T(8,128)(2,1)S(1)}, bf16[608,128]{1,0:T(8,128)(2,1)S(1)}, bf16[608,128]{1,0:T(8,128)(2,1)S(1)}) custom-call(s32[2,64]{1,0:T(2,128)} %bitcast.6, f32[1,64]{1,0:T(1,128)} %bitcast.7, f32[1,64]{1,0:T(1,128)} %bitcast.8, bf16[64,512]{1,0:T(8,128)(2,1)} %refs_3_.1, f32[1,256]{1,0:T(1,128)} %bitcast.4, ...), custom_call_target="tpu_custom_call" | custom-call | tf_op jit(solution)/shard_map/start_first/pallas_call | solution.py:113
  6.6 3.9 %collective-permute-start.5 = (bf16[608,128]{1,0:T(8,128)(2,1)S(1)}, bf16[608,128]{1,0:T(8,128)(2,1)S(1)}, u32[]{:S(2)}, u32[]{:S(2)}) collective-permute-start(bf16[608,128]{1,0:T(8,128)(2,1)S(1)} %get-tuple-element.46), channel_id=1, source_target_pairs={{0,24},{4,28},{8,16},{12,20},{16,8},{20,12},{24,0},{28,4},{1,25},{... | collective-permute-start | bytes 466952 | tf_op jit(solution)/shard_map/ppermute | solution.py:459
  10.5 1.2 %collective-permute-start.6 = (bf16[608,128]{1,0:T(8,128)(2,1)S(1)}, bf16[608,128]{1,0:T(8,128)(2,1)S(1)}, u32[]{:S(2)}, u32[]{:S(2)}) collective-permute-start(bf16[608,128]{1,0:T(8,128)(2,1)S(1)} %get-tuple-element.47), channel_id=1, source_target_pairs={{0,28},{4,24},{8,20},{12,16},{16,12},{20,8},{24,4},{28,0},{1,29},{... | collective-permute-start | bytes 466952 | tf_op jit(solution)/shard_map/ppermute | solution.py:459
  11.7 1.6 %start_later.1 = (bf16[608,128]{1,0:T(8,128)(2,1)S(1)}, bf16[608,128]{1,0:T(8,128)(2,1)S(1)}, bf16[608,128]{1,0:T(8,128)(2,1)S(1)}, bf16[608,128]{1,0:T(8,128)(2...) custom-call(bf16[6,96,128]{2,1,0:T(8,128)(2,1)S(1)} %get-tuple-element.39.rows_ref, ...), custom_call_target="tpu_custom_call" | custom-call | tf_op jit(solution)/shard_map/start_later/pallas_call | solution.py:154
  13.2 1.1 %collective-permute-start = (bf16[608,128]{1,0:T(8,128)(2,1)S(1)}, bf16[608,128]{1,0:T(8,128)(2,1)S(1)}, u32[]{:S(2)}, u32[]{:S(2)}) collective-permute-start(bf16[608,128]{1,0:T(8,128)(2,1)S(1)} %get-tuple-element.41), channel_id=1, source_target_pairs={{0,4},{4,0},{8,12},{12,8},{16,20},{20,16},{24,28},{28,24},{1,5},{5... | collective-permute-start | bytes 466952 | tf_op jit(solution)/shard_map/ppermute | solution.py:459
  14.3 2.5 %collective-permute-start.2 = (bf16[608,128]{1,0:T(8,128)(2,1)S(1)}, bf16[608,128]{1,0:T(8,128)(2,1)S(1)}, u32[]{:S(2)}, u32[]{:S(2)}) collective-permute-start(bf16[608,128]{1,0:T(8,128)(2,1)S(1)} %get-tuple-element.43), channel_id=1, source_target_pairs={{0,12},{4,8},{8,4},{12,0},{16,28},{20,24},{24,20},{28,16},{1,13},{... | collective-permute-start | bytes 466952 | tf_op jit(solution)/shard_map/ppermute | solution.py:459
  16.8 6.2 %collective-permute-start.3 = (bf16[608,128]{1,0:T(8,128)(2,1)S(1)}, bf16[608,128]{1,0:T(8,128)(2,1)S(1)}, u32[]{:S(2)}, u32[]{:S(2)}) collective-permute-start(bf16[608,128]{1,0:T(8,128)(2,1)S(1)} %get-tuple-element.44), channel_id=1, source_target_pairs={{0,16},{4,20},{8,24},{12,28},{16,0},{20,4},{24,8},{28,12},{1,17},{... | collective-permute-start | bytes 466952 | tf_op jit(solution)/shard_map/ppermute | solution.py:459
  23.0 6.0 %collective-permute-start.4 = (bf16[608,128]{1,0:T(8,128)(2,1)S(1)}, bf16[608,128]{1,0:T(8,128)(2,1)S(1)}, u32[]{:S(2)}, u32[]{:S(2)}) collective-permute-start(bf16[608,128]{1,0:T(8,128)(2,1)S(1)} %get-tuple-element.45), channel_id=1, source_target_pairs={{0,20},{4,16},{8,28},{12,24},{16,4},{20,0},{24,12},{28,8},{1,21},{... | collective-permute-start | bytes 466952 | tf_op jit(solution)/shard_map/ppermute | solution.py:459
  29.3 3.3 %collective-permute-start.11 = (bf16[4,64,128]{2,1,0:T(8,128)(2,1)S(1)}, bf16[4,64,128]{2,1,0:T(8,128)(2,1)S(1)}, u32[]{:S(2)}, u32[]{:S(2)}) collective-permute-start(bf16[4,64,128]{2,1,0:T(8,128)(2,1)S(1)} %get-tuple-element.53), channel_id=1, source_target_pairs={{0,8},{4,12},{8,0},{12,4},{16,24},{20,28},{24,16},{28,20},{1,9},{5... | collective-permute-start | bytes 196616 | tf_op jit(solution)/shard_map/ppermute | solution.py:459
  32.6 2.4 %collective-permute-done.3.refs_4_.refs_1_.refs_12_ = bf16[608,128]{1,0:T(8,128)(2,1)S(1)} collective-permute-done((bf16[608,128]{1,0:T(8,128)(2,1)S(1)}, bf16[608,128]{1,0:T(8,128)(2,1)S(1)}, u32[]{:S(2)}, u32[]{:S(2)}) %collective-permute-start.3) | collective-permute-done | bytes 155680 | tf_op jit(solution)/shard_map/ppermute | solution.py:459
  35.0 1.5 %collective-permute-start.17 = (bf16[144,512]{1,0:T(8,128)(2,1)S(1)}, bf16[144,512]{1,0:T(8,128)(2,1)S(1)}, u32[]{:S(2)}, u32[]{:S(2)}) collective-permute-start(bf16[144,512]{1,0:T(8,128)(2,1)S(1)} %slot_rows.2.refs_0_), channel_id=1, source_target_pairs={{0,2},{1,3},{2,0},{3,1},{4,6},{5,7},{6,4},{7,5},{8,10},{9,11},{10,... | collective-permute-start | bytes 442376 | tf_op jit(solution)/shard_map/ppermute | solution.py:464
  36.5 2.2 %collective-permute-done.4.refs_5_.refs_0_.refs_13_ = bf16[608,128]{1,0:T(8,128)(2,1)S(1)} collective-permute-done((bf16[608,128]{1,0:T(8,128)(2,1)S(1)}, bf16[608,128]{1,0:T(8,128)(2,1)S(1)}, u32[]{:S(2)}, u32[]{:S(2)}) %collective-permute-start.4) | collective-permute-done | bytes 155680 | tf_op jit(solution)/shard_map/ppermute | solution.py:459
  39.3 1.1 %collective-permute-start.16 = (bf16[144,512]{1,0:T(8,128)(2,1)S(1)}, bf16[144,512]{1,0:T(8,128)(2,1)S(1)}, u32[]{:S(2)}, u32[]{:S(2)}) collective-permute-start(bf16[144,512]{1,0:T(8,128)(2,1)S(1)} %slot_rows.2.refs_0_), channel_id=1, source_target_pairs={{0,1},{1,0},{2,3},{3,2},{4,5},{5,4},{6,7},{7,6},{8,9},{9,8},{10,11... | collective-permute-start | bytes 442376 | tf_op jit(solution)/shard_map/ppermute | solution.py:464
  40.9 1.8 %collective-permute-done.21.refs_7_ = bf16[48,512]{1,0:T(8,128)(2,1)S(1)} collective-permute-done((bf16[48,512]{1,0:T(8,128)(2,1)S(1)}, bf16[48,512]{1,0:T(8,128)(2,1)S(1)}, u32[]{:S(2)}, u32[]{:S(2)}) %collective-permute-start.21) | collective-permute-done | bytes 49184 | tf_op jit(solution)/shard_map/ppermute | solution.py:464
  42.9 1.6 %collective-permute-done.20.refs_6_ = bf16[48,512]{1,0:T(8,128)(2,1)S(1)} collective-permute-done((bf16[48,512]{1,0:T(8,128)(2,1)S(1)}, bf16[48,512]{1,0:T(8,128)(2,1)S(1)}, u32[]{:S(2)}, u32[]{:S(2)}) %collective-permute-start.20) | collective-permute-done | bytes 49184 | tf_op jit(solution)/shard_map/ppermute | solution.py:464
  45.0 3.8 %collective-permute-start.26 = (bf16[4,64,128]{2,1,0:T(8,128)(2,1)S(1)}, bf16[4,64,128]{2,1,0:T(8,128)(2,1)S(1)}, u32[]{:S(2)}, u32[]{:S(2)}) collective-permute-start(bf16[4,64,128]{2,1,0:T(8,128)(2,1)S(1)} %get-tuple-element.64), channel_id=1, source_target_pairs={{0,20},{4,16},{8,28},{12,24},{16,4},{20,0},{24,12},{28,8},{1,21},{... | collective-permute-start | bytes 196616 | tf_op jit(solution)/shard_map/ppermute | solution.py:459
  48.9 3.4 %collective-permute-start.27 = (bf16[4,64,128]{2,1,0:T(8,128)(2,1)S(1)}, bf16[4,64,128]{2,1,0:T(8,128)(2,1)S(1)}, u32[]{:S(2)}, u32[]{:S(2)}) collective-permute-start(bf16[4,64,128]{2,1,0:T(8,128)(2,1)S(1)} %get-tuple-element.65), channel_id=1, source_target_pairs={{0,24},{4,28},{8,16},{12,20},{16,8},{20,12},{24,0},{28,4},{1,25},{... | collective-permute-start | bytes 196616 | tf_op jit(solution)/shard_map/ppermute | solution.py:459
  53.4 1.0 %collective-permute-start.23 = (bf16[192,128]{1,0:T(8,128)(2,1)S(1)}, bf16[192,128]{1,0:T(8,128)(2,1)S(1)}, u32[]{:S(2)}, u32[]{:S(2)}) collective-permute-start(bf16[192,128]{1,0:T(8,128)(2,1)S(1)} %gate_up.1.refs_0_), channel_id=1, source_target_pairs={{0,2},{1,3},{2,0},{3,1},{4,6},{5,7},{6,4},{7,5},{8,10},{9,11},{10,... | collective-permute-start | bytes 147464 | tf_op jit(solution)/shard_map/ppermute | solution.py:464
  54.4 2.5 %collective-permute-done.26.refs_9_.refs_2_ = bf16[4,64,128]{2,1,0:T(8,128)(2,1)S(1)} collective-permute-done((bf16[4,64,128]{2,1,0:T(8,128)(2,1)S(1)}, bf16[4,64,128]{2,1,0:T(8,128)(2,1)S(1)}, u32[]{:S(2)}, u32[]{:S(2)}) %collective-permute-start.26) | collective-permute-done | bytes 65568 | tf_op jit(solution)/shard_map/ppermute | solution.py:459
  56.9 2.5 %collective-permute-done.28.refs_11_.refs_0_ = bf16[4,64,128]{2,1,0:T(8,128)(2,1)S(1)} collective-permute-done((bf16[4,64,128]{2,1,0:T(8,128)(2,1)S(1)}, bf16[4,64,128]{2,1,0:T(8,128)(2,1)S(1)}, u32[]{:S(2)}, u32[]{:S(2)}) %collective-permute-start.28) | collective-permute-done | bytes 65568 | tf_op jit(solution)/shard_map/ppermute | solution.py:459
  59.4 1.1 %down.1 = bf16[32,24,128]{2,1,0:T(8,128)(2,1)} custom-call(bf16[192,128]{1,0:T(8,128)(2,1)S(1)} %gate_up.1.refs_0_, bf16[192,128]{1,0:T(8,128)(2,1)S(1)} %collective-permute-done.22.refs_1_, bf16[192,128]{1,0:T(8,128)(2,1)S(1)} %collective-permute-done.23.refs_2_, bf16[192,128]{1,0:T(8,128)(2,1)S(1)} %collective-permute-done.24.refs_3_, ...), custom_call_target="tpu_custom_call" | custom-call | tf_op jit(solution)/shard_map/down/pallas_call | solution.py:361
  60.4 3.7 %all-to-all-start = ((bf16[32,24,128]{2,1,0:T(8,128)(2,1)}), bf16[32,24,128]{2,1,0:T(8,128)(2,1)S(1)}, u32[]{:S(2)}, u32[]{:S(2)}) async-start(bf16[32,24,128]{2,1,0:T(8,128)(2,1)} %down.1), calls=%async_computation | async-start | bytes 393216 | tf_op jit(solution)/shard_map/all_to_all | solution.py:509
  64.8 1.8 %collective-permute-start.14 = (bf16[4,64,128]{2,1,0:T(8,128)(2,1)S(1)}, bf16[4,64,128]{2,1,0:T(8,128)(2,1)S(1)}, u32[]{:S(2)}, u32[]{:S(2)}) collective-permute-start(bf16[4,64,128]{2,1,0:T(8,128)(2,1)S(1)} %get-tuple-element.58), channel_id=1, source_target_pairs={{0,2},{1,3},{2,0},{3,1},{4,6},{5,7},{6,4},{7,5},{8,10},{9,11},{10,... | collective-permute-start | bytes 196616 | tf_op jit(solution)/shard_map/ppermute | solution.py:464
  66.6 1.5 %collective-permute-start.30 = (bf16[4,64,128]{2,1,0:T(8,128)(2,1)S(1)}, bf16[4,64,128]{2,1,0:T(8,128)(2,1)S(1)}, u32[]{:S(2)}, u32[]{:S(2)}) collective-permute-start(bf16[4,64,128]{2,1,0:T(8,128)(2,1)S(1)} %get-tuple-element.69), channel_id=1, source_target_pairs={{0,2},{1,3},{2,0},{3,1},{4,6},{5,7},{6,4},{7,5},{8,10},{9,11},{10,... | collective-permute-start | bytes 196616 | tf_op jit(solution)/shard_map/ppermute | solution.py:464
  68.4 2.3 %collective-permute-done.14.refs_10_ = bf16[4,64,128]{2,1,0:T(8,128)(2,1)S(1)} collective-permute-done((bf16[4,64,128]{2,1,0:T(8,128)(2,1)S(1)}, bf16[4,64,128]{2,1,0:T(8,128)(2,1)S(1)}, u32[]{:S(2)}, u32[]{:S(2)}) %collective-permute-start.14) | collective-permute-done | bytes 65568 | tf_op jit(solution)/shard_map/ppermute | solution.py:464
  70.6 1.0 %collective-permute-done.15.refs_11_ = bf16[4,64,128]{2,1,0:T(8,128)(2,1)S(1)} collective-permute-done((bf16[4,64,128]{2,1,0:T(8,128)(2,1)S(1)}, bf16[4,64,128]{2,1,0:T(8,128)(2,1)S(1)}, u32[]{:S(2)}, u32[]{:S(2)}) %collective-permute-start.15) | collective-permute-done | bytes 65568 | tf_op jit(solution)/shard_map/ppermute | solution.py:464
  71.7 1.2 %store.1 = (bf16[1,2048,128]{2,1,0:T(8,128)(2,1)}, bf16[1,2048,128]{2,1,0:T(8,128)(2,1)}, bf16[1,2048,128]{2,1,0:T(8,128)(2,1)}) custom-call(bf16[608,128]{1,0:T(8,128)(2,1)S(1)} %get-tuple-element.40.refs_0_.refs_3_.refs_8_, bf16[608,128]{1,0:T(8,128)(2,1)S(1)} %collective-permute-done.refs_1_.refs_2_.refs_9_, ...), custom_call_target="tpu_custom_call" | custom-call | tf_op jit(solution)/shard_map/store/pallas_call | solution.py:321
  72.9 1.0 %collective-permute-done.30.refs_2_ = bf16[4,64,128]{2,1,0:T(8,128)(2,1)S(1)} collective-permute-done((bf16[4,64,128]{2,1,0:T(8,128)(2,1)S(1)}, bf16[4,64,128]{2,1,0:T(8,128)(2,1)S(1)}, u32[]{:S(2)}, u32[]{:S(2)}) %collective-permute-start.30) | collective-permute-done | bytes 65568 | tf_op jit(solution)/shard_map/ppermute | solution.py:464
  73.9 0.8 %collective-permute-done.31.refs_3_ = bf16[4,64,128]{2,1,0:T(8,128)(2,1)S(1)} collective-permute-done((bf16[4,64,128]{2,1,0:T(8,128)(2,1)S(1)}, bf16[4,64,128]{2,1,0:T(8,128)(2,1)S(1)}, u32[]{:S(2)}, u32[]{:S(2)}) %collective-permute-start.31) | collective-permute-done | bytes 65568 | tf_op jit(solution)/shard_map/ppermute | solution.py:464
  74.7 1.8 %finish.1 = (bf16[64,512]{1,0:T(8,128)(2,1)}, bf16[1,2048,128]{2,1,0:T(8,128)(2,1)}) custom-call(f32[64,6]{1,0:T(8,128)S(1)} %get-tuple-element.62.info_ref, bf16[32,24,128]{2,1,0:T(8,128)(2,1)S(1)} %all-to-all-done.back_ref, bf16[4,64,128]{2,1,0:T(8,128)(2,1)S(1)} %get-tuple-element.67.refs_0_, ...), custom_call_target="tpu_custom_call", output_to_operand_aliasing={{1}: (6, {})} | custom-call | tf_op jit(solution)/shard_map/finish/pallas_call | solution.py:415
  (48 shorter events, 4.7 us)
Async XLA Ops:
  2.0 11.2 %collective-permute-start.7 = (bf16[8,64,128]{2,1,0:T(8,128)(2,1)S(1)}, bf16[8,64,128]{2,1,0:T(8,128)(2,1)S(1)}, u32[]{:S(2)}, u32[]{:S(2)}) collective-permute-start(bf16[8,64,128]{2,1,0:T(8,128)(2,1)S(1)} %get-tuple-element.49), channel_id=1, source_target_pairs={{0,1},{1,0},{2,3},{3,2},{4,5},{5,4},{6,7},{7,6},{8,9},{9,8},{10,11... | collective-permute-start | bytes 393224 | tf_op jit(solution)/shard_map/ppermute | solution.py:464
  2.6 11.8 %collective-permute-start.8 = (bf16[8,64,128]{2,1,0:T(8,128)(2,1)S(1)}, bf16[8,64,128]{2,1,0:T(8,128)(2,1)S(1)}, u32[]{:S(2)}, u32[]{:S(2)}) collective-permute-start(bf16[8,64,128]{2,1,0:T(8,128)(2,1)S(1)} %get-tuple-element.50), channel_id=1, source_target_pairs={{0,2},{1,3},{2,0},{3,1},{4,6},{5,7},{6,4},{7,5},{8,10},{9,11},{10,... | collective-permute-start | bytes 393224 | tf_op jit(solution)/shard_map/ppermute | solution.py:464
  5.1 9.2 %collective-permute-start.9 = (bf16[8,64,128]{2,1,0:T(8,128)(2,1)S(1)}, bf16[8,64,128]{2,1,0:T(8,128)(2,1)S(1)}, u32[]{:S(2)}, u32[]{:S(2)}) collective-permute-start(bf16[8,64,128]{2,1,0:T(8,128)(2,1)S(1)} %get-tuple-element.51), channel_id=1, source_target_pairs={{0,3},{1,2},{2,1},{3,0},{4,7},{5,6},{6,5},{7,4},{8,11},{9,10},{10,... | collective-permute-start | bytes 393224 | tf_op jit(solution)/shard_map/ppermute | solution.py:464
  6.6 10.2 %collective-permute-start.5 = (bf16[608,128]{1,0:T(8,128)(2,1)S(1)}, bf16[608,128]{1,0:T(8,128)(2,1)S(1)}, u32[]{:S(2)}, u32[]{:S(2)}) collective-permute-start(bf16[608,128]{1,0:T(8,128)(2,1)S(1)} %get-tuple-element.46), channel_id=1, source_target_pairs={{0,24},{4,28},{8,16},{12,20},{16,8},{20,12},{24,0},{28,4},{1,25},{... | collective-permute-start | bytes 466952 | tf_op jit(solution)/shard_map/ppermute | solution.py:459
  10.5 12.6 %collective-permute-start.6 = (bf16[608,128]{1,0:T(8,128)(2,1)S(1)}, bf16[608,128]{1,0:T(8,128)(2,1)S(1)}, u32[]{:S(2)}, u32[]{:S(2)}) collective-permute-start(bf16[608,128]{1,0:T(8,128)(2,1)S(1)} %get-tuple-element.47), channel_id=1, source_target_pairs={{0,28},{4,24},{8,20},{12,16},{16,12},{20,8},{24,4},{28,0},{1,29},{... | collective-permute-start | bytes 466952 | tf_op jit(solution)/shard_map/ppermute | solution.py:459
  13.2 15.8 %collective-permute-start = (bf16[608,128]{1,0:T(8,128)(2,1)S(1)}, bf16[608,128]{1,0:T(8,128)(2,1)S(1)}, u32[]{:S(2)}, u32[]{:S(2)}) collective-permute-start(bf16[608,128]{1,0:T(8,128)(2,1)S(1)} %get-tuple-element.41), channel_id=1, source_target_pairs={{0,4},{4,0},{8,12},{12,8},{16,20},{20,16},{24,28},{28,24},{1,5},{5... | collective-permute-start | bytes 466952 | tf_op jit(solution)/shard_map/ppermute | solution.py:459
  14.3 14.8 %collective-permute-start.1 = (bf16[608,128]{1,0:T(8,128)(2,1)S(1)}, bf16[608,128]{1,0:T(8,128)(2,1)S(1)}, u32[]{:S(2)}, u32[]{:S(2)}) collective-permute-start(bf16[608,128]{1,0:T(8,128)(2,1)S(1)} %get-tuple-element.42), channel_id=1, source_target_pairs={{0,8},{4,12},{8,0},{12,4},{16,24},{20,28},{24,16},{28,20},{1,9},{5... | collective-permute-start | bytes 466952 | tf_op jit(solution)/shard_map/ppermute | solution.py:459
  14.3 14.8 %collective-permute-start.2 = (bf16[608,128]{1,0:T(8,128)(2,1)S(1)}, bf16[608,128]{1,0:T(8,128)(2,1)S(1)}, u32[]{:S(2)}, u32[]{:S(2)}) collective-permute-start(bf16[608,128]{1,0:T(8,128)(2,1)S(1)} %get-tuple-element.43), channel_id=1, source_target_pairs={{0,12},{4,8},{8,4},{12,0},{16,28},{20,24},{24,20},{28,16},{1,13},{... | collective-permute-start | bytes 466952 | tf_op jit(solution)/shard_map/ppermute | solution.py:459
  16.8 18.2 %collective-permute-start.3 = (bf16[608,128]{1,0:T(8,128)(2,1)S(1)}, bf16[608,128]{1,0:T(8,128)(2,1)S(1)}, u32[]{:S(2)}, u32[]{:S(2)}) collective-permute-start(bf16[608,128]{1,0:T(8,128)(2,1)S(1)} %get-tuple-element.44), channel_id=1, source_target_pairs={{0,16},{4,20},{8,24},{12,28},{16,0},{20,4},{24,8},{28,12},{1,17},{... | collective-permute-start | bytes 466952 | tf_op jit(solution)/shard_map/ppermute | solution.py:459
  23.0 15.6 %collective-permute-start.4 = (bf16[608,128]{1,0:T(8,128)(2,1)S(1)}, bf16[608,128]{1,0:T(8,128)(2,1)S(1)}, u32[]{:S(2)}, u32[]{:S(2)}) collective-permute-start(bf16[608,128]{1,0:T(8,128)(2,1)S(1)} %get-tuple-element.45), channel_id=1, source_target_pairs={{0,20},{4,16},{8,28},{12,24},{16,4},{20,0},{24,12},{28,8},{1,21},{... | collective-permute-start | bytes 466952 | tf_op jit(solution)/shard_map/ppermute | solution.py:459
  29.1 10.2 %collective-permute-start.10 = (bf16[4,64,128]{2,1,0:T(8,128)(2,1)S(1)}, bf16[4,64,128]{2,1,0:T(8,128)(2,1)S(1)}, u32[]{:S(2)}, u32[]{:S(2)}) collective-permute-start(bf16[4,64,128]{2,1,0:T(8,128)(2,1)S(1)} %get-tuple-element.52), channel_id=1, source_target_pairs={{0,12},{4,8},{8,4},{12,0},{16,28},{20,24},{24,20},{28,16},{1,13},{... | collective-permute-start | bytes 196616 | tf_op jit(solution)/shard_map/ppermute | solution.py:459
  29.2 15.8 %collective-permute-start.18 = (bf16[144,512]{1,0:T(8,128)(2,1)S(1)}, bf16[144,512]{1,0:T(8,128)(2,1)S(1)}, u32[]{:S(2)}, u32[]{:S(2)}) collective-permute-start(bf16[144,512]{1,0:T(8,128)(2,1)S(1)} %slot_rows.2.refs_0_), channel_id=1, source_target_pairs={{0,3},{1,2},{2,1},{3,0},{4,7},{5,6},{6,5},{7,4},{8,11},{9,10},{10,... | collective-permute-start | bytes 442376 | tf_op jit(solution)/shard_map/ppermute | solution.py:464
  29.3 11.1 %collective-permute-start.11 = (bf16[4,64,128]{2,1,0:T(8,128)(2,1)S(1)}, bf16[4,64,128]{2,1,0:T(8,128)(2,1)S(1)}, u32[]{:S(2)}, u32[]{:S(2)}) collective-permute-start(bf16[4,64,128]{2,1,0:T(8,128)(2,1)S(1)} %get-tuple-element.53), channel_id=1, source_target_pairs={{0,8},{4,12},{8,0},{12,4},{16,24},{20,28},{24,16},{28,20},{1,9},{5... | collective-permute-start | bytes 196616 | tf_op jit(solution)/shard_map/ppermute | solution.py:459
  35.0 13.9 %collective-permute-start.17 = (bf16[144,512]{1,0:T(8,128)(2,1)S(1)}, bf16[144,512]{1,0:T(8,128)(2,1)S(1)}, u32[]{:S(2)}, u32[]{:S(2)}) collective-permute-start(bf16[144,512]{1,0:T(8,128)(2,1)S(1)} %slot_rows.2.refs_0_), channel_id=1, source_target_pairs={{0,2},{1,3},{2,0},{3,1},{4,6},{5,7},{6,4},{7,5},{8,10},{9,11},{10,... | collective-permute-start | bytes 442376 | tf_op jit(solution)/shard_map/ppermute | solution.py:464
  38.7 4.1 %collective-permute-start.21 = (bf16[48,512]{1,0:T(8,128)(2,1)S(1)}, bf16[48,512]{1,0:T(8,128)(2,1)S(1)}, u32[]{:S(2)}, u32[]{:S(2)}) collective-permute-start(bf16[48,512]{1,0:T(8,128)(2,1)S(1)} %slot_rows.3.refs_4_), channel_id=1, source_target_pairs={{0,3},{1,2},{2,1},{3,0},{4,7},{5,6},{6,5},{7,4},{8,11},{9,10},{10,... | collective-permute-start | bytes 147464 | tf_op jit(solution)/shard_map/ppermute | solution.py:464
  39.3 13.0 %collective-permute-start.16 = (bf16[144,512]{1,0:T(8,128)(2,1)S(1)}, bf16[144,512]{1,0:T(8,128)(2,1)S(1)}, u32[]{:S(2)}, u32[]{:S(2)}) collective-permute-start(bf16[144,512]{1,0:T(8,128)(2,1)S(1)} %slot_rows.2.refs_0_), channel_id=1, source_target_pairs={{0,1},{1,0},{2,3},{3,2},{4,5},{5,4},{6,7},{7,6},{8,9},{9,8},{10,11... | collective-permute-start | bytes 442376 | tf_op jit(solution)/shard_map/ppermute | solution.py:464
  40.4 4.1 %collective-permute-start.20 = (bf16[48,512]{1,0:T(8,128)(2,1)S(1)}, bf16[48,512]{1,0:T(8,128)(2,1)S(1)}, u32[]{:S(2)}, u32[]{:S(2)}) collective-permute-start(bf16[48,512]{1,0:T(8,128)(2,1)S(1)} %slot_rows.3.refs_4_), channel_id=1, source_target_pairs={{0,2},{1,3},{2,0},{3,1},{4,6},{5,7},{6,4},{7,5},{8,10},{9,11},{10,... | collective-permute-start | bytes 147464 | tf_op jit(solution)/shard_map/ppermute | solution.py:464
  44.5 8.8 %collective-permute-start.12 = (bf16[4,64,128]{2,1,0:T(8,128)(2,1)S(1)}, bf16[4,64,128]{2,1,0:T(8,128)(2,1)S(1)}, u32[]{:S(2)}, u32[]{:S(2)}) collective-permute-start(bf16[4,64,128]{2,1,0:T(8,128)(2,1)S(1)} %get-tuple-element.54), channel_id=1, source_target_pairs={{0,4},{4,0},{8,12},{12,8},{16,20},{20,16},{24,28},{28,24},{1,5},{5... | collective-permute-start | bytes 196616 | tf_op jit(solution)/shard_map/ppermute | solution.py:459
  45.0 8.4 %collective-permute-start.25 = (bf16[4,64,128]{2,1,0:T(8,128)(2,1)S(1)}, bf16[4,64,128]{2,1,0:T(8,128)(2,1)S(1)}, u32[]{:S(2)}, u32[]{:S(2)}) collective-permute-start(bf16[4,64,128]{2,1,0:T(8,128)(2,1)S(1)} %get-tuple-element.63), channel_id=1, source_target_pairs={{0,16},{4,20},{8,24},{12,28},{16,0},{20,4},{24,8},{28,12},{1,17},{... | collective-permute-start | bytes 196616 | tf_op jit(solution)/shard_map/ppermute | solution.py:459
  45.0 11.9 %collective-permute-start.26 = (bf16[4,64,128]{2,1,0:T(8,128)(2,1)S(1)}, bf16[4,64,128]{2,1,0:T(8,128)(2,1)S(1)}, u32[]{:S(2)}, u32[]{:S(2)}) collective-permute-start(bf16[4,64,128]{2,1,0:T(8,128)(2,1)S(1)} %get-tuple-element.64), channel_id=1, source_target_pairs={{0,20},{4,16},{8,28},{12,24},{16,4},{20,0},{24,12},{28,8},{1,21},{... | collective-permute-start | bytes 196616 | tf_op jit(solution)/shard_map/ppermute | solution.py:459
  48.9 8.0 %collective-permute-start.27 = (bf16[4,64,128]{2,1,0:T(8,128)(2,1)S(1)}, bf16[4,64,128]{2,1,0:T(8,128)(2,1)S(1)}, u32[]{:S(2)}, u32[]{:S(2)}) collective-permute-start(bf16[4,64,128]{2,1,0:T(8,128)(2,1)S(1)} %get-tuple-element.65), channel_id=1, source_target_pairs={{0,24},{4,28},{8,16},{12,20},{16,8},{20,12},{24,0},{28,4},{1,25},{... | collective-permute-start | bytes 196616 | tf_op jit(solution)/shard_map/ppermute | solution.py:459
  52.3 7.1 %collective-permute-start.28 = (bf16[4,64,128]{2,1,0:T(8,128)(2,1)S(1)}, bf16[4,64,128]{2,1,0:T(8,128)(2,1)S(1)}, u32[]{:S(2)}, u32[]{:S(2)}) collective-permute-start(bf16[4,64,128]{2,1,0:T(8,128)(2,1)S(1)} %get-tuple-element.66), channel_id=1, source_target_pairs={{0,28},{4,24},{8,20},{12,16},{16,12},{20,8},{24,4},{28,0},{1,29},{... | collective-permute-start | bytes 196616 | tf_op jit(solution)/shard_map/ppermute | solution.py:459
  53.3 6.1 %collective-permute-start.24 = (bf16[192,128]{1,0:T(8,128)(2,1)S(1)}, bf16[192,128]{1,0:T(8,128)(2,1)S(1)}, u32[]{:S(2)}, u32[]{:S(2)}) collective-permute-start(bf16[192,128]{1,0:T(8,128)(2,1)S(1)} %gate_up.1.refs_0_), channel_id=1, source_target_pairs={{0,3},{1,2},{2,1},{3,0},{4,7},{5,6},{6,5},{7,4},{8,11},{9,10},{10,... | collective-permute-start | bytes 147464 | tf_op jit(solution)/shard_map/ppermute | solution.py:464
  53.4 6.0 %collective-permute-start.23 = (bf16[192,128]{1,0:T(8,128)(2,1)S(1)}, bf16[192,128]{1,0:T(8,128)(2,1)S(1)}, u32[]{:S(2)}, u32[]{:S(2)}) collective-permute-start(bf16[192,128]{1,0:T(8,128)(2,1)S(1)} %gate_up.1.refs_0_), channel_id=1, source_target_pairs={{0,2},{1,3},{2,0},{3,1},{4,6},{5,7},{6,4},{7,5},{8,10},{9,11},{10,... | collective-permute-start | bytes 147464 | tf_op jit(solution)/shard_map/ppermute | solution.py:464
  56.9 2.5 %collective-permute-start.22 = (bf16[192,128]{1,0:T(8,128)(2,1)S(1)}, bf16[192,128]{1,0:T(8,128)(2,1)S(1)}, u32[]{:S(2)}, u32[]{:S(2)}) collective-permute-start(bf16[192,128]{1,0:T(8,128)(2,1)S(1)} %gate_up.1.refs_0_), channel_id=1, source_target_pairs={{0,1},{1,0},{2,3},{3,2},{4,5},{5,4},{6,7},{7,6},{8,9},{9,8},{10,11... | collective-permute-start | bytes 147464 | tf_op jit(solution)/shard_map/ppermute | solution.py:464
  60.4 14.3 %all-to-all-start = ((bf16[32,24,128]{2,1,0:T(8,128)(2,1)}), bf16[32,24,128]{2,1,0:T(8,128)(2,1)S(1)}, u32[]{:S(2)}, u32[]{:S(2)}) async-start(bf16[32,24,128]{2,1,0:T(8,128)(2,1)} %down.1), calls=%async_computation | async-start | bytes 393216 | tf_op jit(solution)/shard_map/all_to_all | solution.py:509
  64.2 3.9 %collective-permute-start.13 = (bf16[4,64,128]{2,1,0:T(8,128)(2,1)S(1)}, bf16[4,64,128]{2,1,0:T(8,128)(2,1)S(1)}, u32[]{:S(2)}, u32[]{:S(2)}) collective-permute-start(bf16[4,64,128]{2,1,0:T(8,128)(2,1)S(1)} %get-tuple-element.57), channel_id=1, source_target_pairs={{0,1},{1,0},{2,3},{3,2},{4,5},{5,4},{6,7},{7,6},{8,9},{9,8},{10,11... | collective-permute-start | bytes 196616 | tf_op jit(solution)/shard_map/ppermute | solution.py:464
  64.5 8.4 %collective-permute-start.29 = (bf16[4,64,128]{2,1,0:T(8,128)(2,1)S(1)}, bf16[4,64,128]{2,1,0:T(8,128)(2,1)S(1)}, u32[]{:S(2)}, u32[]{:S(2)}) collective-permute-start(bf16[4,64,128]{2,1,0:T(8,128)(2,1)S(1)} %get-tuple-element.68), channel_id=1, source_target_pairs={{0,1},{1,0},{2,3},{3,2},{4,5},{5,4},{6,7},{7,6},{8,9},{9,8},{10,11... | collective-permute-start | bytes 196616 | tf_op jit(solution)/shard_map/ppermute | solution.py:464
  64.8 5.8 %collective-permute-start.14 = (bf16[4,64,128]{2,1,0:T(8,128)(2,1)S(1)}, bf16[4,64,128]{2,1,0:T(8,128)(2,1)S(1)}, u32[]{:S(2)}, u32[]{:S(2)}) collective-permute-start(bf16[4,64,128]{2,1,0:T(8,128)(2,1)S(1)} %get-tuple-element.58), channel_id=1, source_target_pairs={{0,2},{1,3},{2,0},{3,1},{4,6},{5,7},{6,4},{7,5},{8,10},{9,11},{10,... | collective-permute-start | bytes 196616 | tf_op jit(solution)/shard_map/ppermute | solution.py:464
  66.6 5.0 %collective-permute-start.15 = (bf16[4,64,128]{2,1,0:T(8,128)(2,1)S(1)}, bf16[4,64,128]{2,1,0:T(8,128)(2,1)S(1)}, u32[]{:S(2)}, u32[]{:S(2)}) collective-permute-start(bf16[4,64,128]{2,1,0:T(8,128)(2,1)S(1)} %get-tuple-element.59), channel_id=1, source_target_pairs={{0,3},{1,2},{2,1},{3,0},{4,7},{5,6},{6,5},{7,4},{8,11},{9,10},{10,... | collective-permute-start | bytes 196616 | tf_op jit(solution)/shard_map/ppermute | solution.py:464
  66.6 7.3 %collective-permute-start.30 = (bf16[4,64,128]{2,1,0:T(8,128)(2,1)S(1)}, bf16[4,64,128]{2,1,0:T(8,128)(2,1)S(1)}, u32[]{:S(2)}, u32[]{:S(2)}) collective-permute-start(bf16[4,64,128]{2,1,0:T(8,128)(2,1)S(1)} %get-tuple-element.69), channel_id=1, source_target_pairs={{0,2},{1,3},{2,0},{3,1},{4,6},{5,7},{6,4},{7,5},{8,10},{9,11},{10,... | collective-permute-start | bytes 196616 | tf_op jit(solution)/shard_map/ppermute | solution.py:464
  68.1 6.6 %collective-permute-start.31 = (bf16[4,64,128]{2,1,0:T(8,128)(2,1)S(1)}, bf16[4,64,128]{2,1,0:T(8,128)(2,1)S(1)}, u32[]{:S(2)}, u32[]{:S(2)}) collective-permute-start(bf16[4,64,128]{2,1,0:T(8,128)(2,1)S(1)} %get-tuple-element.70), channel_id=1, source_target_pairs={{0,3},{1,2},{2,1},{3,0},{4,7},{5,6},{6,5},{7,4},{8,11},{9,10},{10,... | collective-permute-start | bytes 196616 | tf_op jit(solution)/shard_map/ppermute | solution.py:464
  (2 other events, 3.4 us)

commit v2 on v1

--- a/solution.py
+++ b/solution.py
@@ -342,30 +342,41 @@
     def kernel(*refs):
         hidden_refs = refs[:n_tp]
         chunk_refs = refs[n_tp : n_tp + n_fs]
-        out_ref, hidden_ref, all_ref = refs[n_tp + n_fs :]
+        out_ref, hidden_ref, all_ref, value_ref, sems = refs[n_tp + n_fs :]
         own, _ = own_places()
+        wide = ratio * part
         for t in range(n_tp):
             hidden_ref[:, t * cols : (t + 1) * cols] = hidden_refs[t][...]
-            for s in range(n_fs):
-                all_ref[s * part : (s + 1) * part, t * cols : (t + 1) * cols] = chunk_refs[s][t]
-        total = lax.dot_general(
-            hidden_ref[...], all_ref[...], (((1,), (1,)), ((), ())), preferred_element_type=F32
-        )
-        wide = ratio * part
+        copies = []
         for m in range(n_tp):
+            for s in range(m * ratio, (m + 1) * ratio):
+                for t in range(n_tp):
+                    all_ref[s * part : (s + 1) * part, t * cols : (t + 1) * cols] = chunk_refs[s][t]
+            value = lax.dot_general(
+                hidden_ref[...],
+                all_ref[m * wide : (m + 1) * wide],
+                (((1,), (1,)), ((), ())),
+                preferred_element_type=F32,
+            )
             for k, s in enumerate(row_order):
-                out_ref[(own ^ s) * n_tp + ((own // ratio) ^ m)] = total[
-                    k * capacity : (k + 1) * capacity, m * wide : (m + 1) * wide
-                ].astype(BF16)
+                value_ref[m, own ^ s] = value[k * capacity : (k + 1) * capacity].astype(BF16)
+            quarter = (own // ratio) ^ m
+            copy = pltpu.make_async_copy(value_ref.at[m], out_ref.at[:, quarter], sems.at[m])
+            copy.start()
+            copies.append(copy)
+        for copy in copies:
+            copy.wait()
 
     return pl.pallas_call(
         kernel,
         in_specs=[whole(VMEM)] * (n_tp + n_fs),
-        out_specs=whole(VMEM),
-        out_shape=jax.ShapeDtypeStruct((n_fs * n_tp, capacity, ratio * part), BF16),
+        out_specs=whole(ANY),
+        out_shape=jax.ShapeDtypeStruct((n_fs, n_tp, capacity, ratio * part), BF16),
         scratch_shapes=[
             VMEM((slots, n_tp * cols), BF16),
             VMEM((n_fs * part, n_tp * cols), BF16),
+            VMEM((n_tp, n_fs, capacity, ratio * part), BF16),
+            pltpu.SemaphoreType.DMA((n_tp,)),
         ],
         compiler_params=GRANT,
         name="down",
@@ -382,7 +393,7 @@
 
     def kernel(info_ref, back_ref, *refs):
         piece_refs = refs[:n_tp]
-        out, down_ref, block_ref, back_rows, sems = refs[n_tp + 1 :]
+        mixed_ref, down_ref, block_ref, back_rows, out, sems, out_sem = refs[n_tp + 1 :]
         own, lane = own_places()
         copies = gather_blocks(batch, piece_refs, own, lane, block_ref, down_ref, sems)
         for e in range(n_fs):
@@ -409,13 +420,14 @@
                 value = values[:, 0:1] * total[:rows] + values[:, 1:2] * total[rows:]
                 at = (y * n_tp + j) * part
                 out[:, at : at + part] = value.astype(BF16)
+        copies += fetch([(out, mixed_ref)], out_sem)
         for copy in copies:
             copy.wait()
 
     return pl.pallas_call(
         kernel,
         in_specs=[whole(VMEM)] * (2 + n_tp) + [whole(ANY)],
-        out_specs=[whole(VMEM), whole(ANY)],
+        out_specs=[whole(ANY), whole(ANY)],
         out_shape=[
             jax.ShapeDtypeStruct((rows, n_tp * wide), BF16),
             jax.ShapeDtypeStruct(down_half.shape, BF16),
@@ -423,7 +435,9 @@
         scratch_shapes=[
             VMEM((len(batch), n_tp * part, cols), BF16),
             VMEM((ratio, group * capacity, n_tp * wide), BF16),
+            VMEM((rows, n_tp * wide), BF16),
             pltpu.SemaphoreType.DMA((len(batch),)),
+            pltpu.SemaphoreType.DMA((1,)),
         ],
         input_output_aliases={2 + n_tp: 1},
         compiler_params=GRANT,
@@ -463,6 +477,15 @@
             return value
         return lax.ppermute(value, "tp", [(n, n ^ s) for n in range(n_tp)])
 
+    def gather_tp(value):
+        parts = {0: value}
+        step = n_tp
+        while step > 1:
+            step //= 2
+            for t in sorted(parts):
+                parts[t + step] = lax.ppermute(parts[t], "tp", [(n, n ^ step) for n in range(n_tp)])
+        return [parts[t] for t in range(n_tp)]
+
     gain = norm_gain[None, :]
     gate_weight, up_weight, down_weight = (
         pltpu.with_memory_space_constraint(value, pltpu.HBM)
@@ -498,17 +521,18 @@
     parts, quarters = [], []
     for batch in batches:
         rows = slot_rows_of([chunks[s] for s in batch], 2 * block, capacity)
-        parts.append([swap_tp(rows, t) for t in range(n_tp)])
-    for batch in (near, far):
+        parts.append(gather_tp(rows))
+    for batch in batches:
         pieces = regroup([down_chunks[s] for s in batch])
         quarters.append([swap_tp(pieces[t], t) for t in range(n_tp)])
 
     hidden = gate_up(parts, chunks, block)
-    hiddens = [swap_tp(hidden, t) for t in range(n_tp)]
+    hiddens = gather_tp(hidden)
     rows = down(row_order, hiddens, down_chunks, capacity)
+    rows = rows.reshape(n_fs * n_tp, *rows.shape[2:])
     back = lax.all_to_all(rows, ("fs", "tp"), split_axis=0, concat_axis=0, tiled=True)
-    gate_out, up_out, down_half = store(chunks, block, near, quarters[0])
-    mixed, down_out = finish(info, back, n_fs, far, quarters[1], down_half)
+    gate_out, up_out, down_half = store(chunks, block, batches[0], quarters[0])
+    mixed, down_out = finish(info, back, n_fs, batches[1], quarters[1], down_half)
     return gate_out, up_out, down_out, mixed
 
 

time: 76.8 us -> 81.9 us (1.066)
  waiting for transfers between devices: 18.1 us -> 33.3 us
  starting transfers between devices: 48.4 us -> 38 us
    ppermute x14, waiting for transfers between devices: 9.57 us -> 25.8 us  [swap_fs(): return lax.ppermute(value, 'fs', [(n, n ^ s) for n in range(n_fs)])]
    ppermute x18 -> x9, starting transfers between devices: 12.3 us -> 4.82 us  [swap_tp(): return lax.ppermute(value, 'tp', [(n, n ^ s) for n in range(n_tp)])]
    ppermute x14, starting transfers between devices: 32.4 us -> 25.7 us  [swap_fs(): return lax.ppermute(value, 'fs', [(n, n ^ s) for n in range(n_fs)])]
    ppermute x0 -> x9, starting transfers between devices: none -> 4.82 us  [gather_tp(): lax.ppermute(parts[t], 'tp', [(n, n ^ step) for n in range(n_tp)])]
    ppermute x18 -> x9, waiting for transfers between devices: 8.57 us -> 4.84 us  [swap_tp(): return lax.ppermute(value, 'tp', [(n, n ^ s) for n in range(n_tp)])]
    ppermute x0 -> x9, waiting for transfers between devices: none -> 2.61 us  [gather_tp(): lax.ppermute(parts[t], 'tp', [(n, n ^ step) for n in range(n_tp)])]
    all_to_all x1, starting transfers between devices: 3.7 us -> 2.61 us  [exchange_body(): lax.all_to_all(rows, ('fs', 'tp'), split_axis=0, concat_axis=0, tiled=True)]
  transfers between devices with their start and end apart: 33 -> 33, of which waited for: 10 -> 11; matrix products, arithmetic and copies ran while one was open for 0% -> 0% of each run, Pallas kernels for 6% -> 4%
where the time goes in v2:
time: 81.9 us; the launch traced here: 81.3 us
  starting transfers between devices  38 us (46%)
  waiting for transfers between devices  33.3 us (41%)
  Pallas kernels  8.58 us (10%)
    ppermute x14, waiting for transfers between devices, swap_fs(): return lax.ppermute(value, 'fs', [(n, n ^ s) for n in range(n_fs)])  25.8 us
    ppermute x14, starting transfers between devices, swap_fs(): return lax.ppermute(value, 'fs', [(n, n ^ s) for n in range(n_fs)])  25.7 us
    ppermute x9, waiting for transfers between devices, swap_tp(): return lax.ppermute(value, 'tp', [(n, n ^ s) for n in range(n_tp)])  4.84 us
    ppermute x9, starting transfers between devices, swap_tp(): return lax.ppermute(value, 'tp', [(n, n ^ s) for n in range(n_tp)])  4.82 us
    ppermute x9, starting transfers between devices, gather_tp(): lax.ppermute(parts[t], 'tp', [(n, n ^ step) for n in range(n_tp)])  4.82 us
    ppermute x9, waiting for transfers between devices, gather_tp(): lax.ppermute(parts[t], 'tp', [(n, n ^ step) for n in range(n_tp)])  2.61 us
    all_to_all x1, starting transfers between devices, exchange_body(): lax.all_to_all(rows, ('fs', 'tp'), split_axis=0, concat_axis=0, tiled=True)  2.61 us
  transfers between devices with their start and end apart: 33, of which 11 were waited for; matrix products, arithmetic and copies ran while one was open for 0% of the time, Pallas kernels for 4%

profile of v2, /device:TPU:0, one launch (start us, length us, event | category | flops | bytes accessed | tf_op | source)
XLA Modules:
  0.0 81.3 jit_solution(14562910333112953378)
XLA Ops:
  0.6 1.4 %start_first.1 = (f32[64,6]{1,0:T(8,128)S(1)}, bf16[6,96,128]{2,1,0:T(8,128)(2,1)S(1)}, bf16[608,128]{1,0:T(8,128)(2,1)S(1)}, bf16[608,128]{1,0:T(8,128)(2,1)S(1)}) custom-call(s32[2,64]{1,0:T(2,128)} %bitcast.7, f32[1,64]{1,0:T(1,128)} %bitcast.8, f32[1,64]{1,0:T(1,128)} %bitcast.9, bf16[64,512]{1,0:T(8,128)(2,1)} %refs_3_.1, f32[1,256]{1,0:T(1,128)} %bitcast.5, ...), custom_call_target="tpu_custom_call" | custom-call | tf_op jit(solution)/shard_map/start_first/pallas_call | solution.py:113
  2.7 1.6 %start_later.1 = (bf16[608,128]{1,0:T(8,128)(2,1)S(1)}, bf16[608,128]{1,0:T(8,128)(2,1)S(1)}, bf16[608,128]{1,0:T(8,128)(2,1)S(1)}, bf16[608,128]{1,0:T(8,128)(2...) custom-call(bf16[6,96,128]{2,1,0:T(8,128)(2,1)S(1)} %get-tuple-element.39.rows_ref, ...), custom_call_target="tpu_custom_call" | custom-call | tf_op jit(solution)/shard_map/start_later/pallas_call | solution.py:154
  4.3 3.1 %collective-permute-start = (bf16[608,128]{1,0:T(8,128)(2,1)S(1)}, bf16[608,128]{1,0:T(8,128)(2,1)S(1)}, u32[]{:S(2)}, u32[]{:S(2)}) collective-permute-start(bf16[608,128]{1,0:T(8,128)(2,1)S(1)} %get-tuple-element.41), channel_id=1, source_target_pairs={{0,4},{4,0},{8,12},{12,8},{16,20},{20,16},{24,28},{28,24},{1,5},{5... | collective-permute-start | bytes 466952 | tf_op jit(solution)/shard_map/ppermute | solution.py:473
  7.4 1.6 %collective-permute-start.1 = (bf16[608,128]{1,0:T(8,128)(2,1)S(1)}, bf16[608,128]{1,0:T(8,128)(2,1)S(1)}, u32[]{:S(2)}, u32[]{:S(2)}) collective-permute-start(bf16[608,128]{1,0:T(8,128)(2,1)S(1)} %get-tuple-element.42), channel_id=1, source_target_pairs={{0,8},{4,12},{8,0},{12,4},{16,24},{20,28},{24,16},{28,20},{1,9},{5... | collective-permute-start | bytes 466952 | tf_op jit(solution)/shard_map/ppermute | solution.py:473
  8.9 4.0 %collective-permute-start.5 = (bf16[608,128]{1,0:T(8,128)(2,1)S(1)}, bf16[608,128]{1,0:T(8,128)(2,1)S(1)}, u32[]{:S(2)}, u32[]{:S(2)}) collective-permute-start(bf16[608,128]{1,0:T(8,128)(2,1)S(1)} %get-tuple-element.46), channel_id=1, source_target_pairs={{0,24},{4,28},{8,16},{12,20},{16,8},{20,12},{24,0},{28,4},{1,25},{... | collective-permute-start | bytes 466952 | tf_op jit(solution)/shard_map/ppermute | solution.py:473
  12.9 1.2 %collective-permute-start.6 = (bf16[608,128]{1,0:T(8,128)(2,1)S(1)}, bf16[608,128]{1,0:T(8,128)(2,1)S(1)}, u32[]{:S(2)}, u32[]{:S(2)}) collective-permute-start(bf16[608,128]{1,0:T(8,128)(2,1)S(1)} %get-tuple-element.47), channel_id=1, source_target_pairs={{0,28},{4,24},{8,20},{12,16},{16,12},{20,8},{24,4},{28,0},{1,29},{... | collective-permute-start | bytes 466952 | tf_op jit(solution)/shard_map/ppermute | solution.py:473
  14.1 0.8 collective-permute-start.3
  14.9 1.9 %collective-permute-start.4 = (bf16[608,128]{1,0:T(8,128)(2,1)S(1)}, bf16[608,128]{1,0:T(8,128)(2,1)S(1)}, u32[]{:S(2)}, u32[]{:S(2)}) collective-permute-start(bf16[608,128]{1,0:T(8,128)(2,1)S(1)} %get-tuple-element.45), channel_id=1, source_target_pairs={{0,20},{4,16},{8,28},{12,24},{16,4},{20,0},{24,12},{28,8},{1,21},{... | collective-permute-start | bytes 466952 | tf_op jit(solution)/shard_map/ppermute | solution.py:473
  16.8 6.2 %collective-permute-done.5.refs_6_.refs_5_.refs_14_ = bf16[608,128]{1,0:T(8,128)(2,1)S(1)} collective-permute-done((bf16[608,128]{1,0:T(8,128)(2,1)S(1)}, bf16[608,128]{1,0:T(8,128)(2,1)S(1)}, u32[]{:S(2)}, u32[]{:S(2)}) %collective-permute-start.5) | collective-permute-done | bytes 155680 | tf_op jit(solution)/shard_map/ppermute | solution.py:473
  23.0 3.1 %collective-permute-done.6.refs_7_.refs_4_.refs_15_ = bf16[608,128]{1,0:T(8,128)(2,1)S(1)} collective-permute-done((bf16[608,128]{1,0:T(8,128)(2,1)S(1)}, bf16[608,128]{1,0:T(8,128)(2,1)S(1)}, u32[]{:S(2)}, u32[]{:S(2)}) %collective-permute-start.6) | collective-permute-done | bytes 155680 | tf_op jit(solution)/shard_map/ppermute | solution.py:473
  26.2 1.6 %collective-permute-start.19 = (bf16[144,512]{1,0:T(8,128)(2,1)S(1)}, bf16[144,512]{1,0:T(8,128)(2,1)S(1)}, u32[]{:S(2)}, u32[]{:S(2)}) collective-permute-start(bf16[144,512]{1,0:T(8,128)(2,1)S(1)} %slot_rows.2.refs_0_), channel_id=1, source_target_pairs={{0,2},{1,3},{2,0},{3,1},{4,6},{5,7},{6,4},{7,5},{8,10},{9,11},{10,... | collective-permute-start | bytes 442376 | tf_op jit(solution)/shard_map/ppermute | solution.py:486
  27.8 1.4 %cast_rows.1 = (bf16[8,64,128]{2,1,0:T(8,128)(2,1)S(1)}, bf16[8,64,128]{2,1,0:T(8,128)(2,1)S(1)}, bf16[8,64,128]{2,1,0:T(8,128)(2,1)S(1)}, bf16[8,64,128]{2,1,0:T(8,128)(2,1)S(1)}) custom-call(f32[8,256,128]{2,1,0:T(8,128)} %source.1), custom_call_target="tpu_custom_call" | custom-call | tf_op jit(solution)/shard_map/cast_rows/pallas_call | solution.py:207
  29.8 7.1 %collective-permute-done.3.refs_4_.refs_1_.refs_12_ = bf16[608,128]{1,0:T(8,128)(2,1)S(1)} collective-permute-done((bf16[608,128]{1,0:T(8,128)(2,1)S(1)}, bf16[608,128]{1,0:T(8,128)(2,1)S(1)}, u32[]{:S(2)}, u32[]{:S(2)}) %collective-permute-start.3) | collective-permute-done | bytes 155680 | tf_op jit(solution)/shard_map/ppermute | solution.py:473
  37.0 2.6 %collective-permute-done.4.refs_5_.refs_0_.refs_13_ = bf16[608,128]{1,0:T(8,128)(2,1)S(1)} collective-permute-done((bf16[608,128]{1,0:T(8,128)(2,1)S(1)}, bf16[608,128]{1,0:T(8,128)(2,1)S(1)}, u32[]{:S(2)}, u32[]{:S(2)}) %collective-permute-start.4) | collective-permute-done | bytes 155680 | tf_op jit(solution)/shard_map/ppermute | solution.py:473
  40.1 1.6 %collective-permute-start.22 = (bf16[48,512]{1,0:T(8,128)(2,1)S(1)}, bf16[48,512]{1,0:T(8,128)(2,1)S(1)}, u32[]{:S(2)}, u32[]{:S(2)}) collective-permute-start(bf16[48,512]{1,0:T(8,128)(2,1)S(1)} %slot_rows.3.refs_4_), channel_id=1, source_target_pairs={{0,2},{1,3},{2,0},{3,1},{4,6},{5,7},{6,4},{7,5},{8,10},{9,11},{10,... | collective-permute-start | bytes 147464 | tf_op jit(solution)/shard_map/ppermute | solution.py:486
  41.7 2.6 %collective-permute-done.22.refs_6_ = bf16[48,512]{1,0:T(8,128)(2,1)S(1)} collective-permute-done((bf16[48,512]{1,0:T(8,128)(2,1)S(1)}, bf16[48,512]{1,0:T(8,128)(2,1)S(1)}, u32[]{:S(2)}, u32[]{:S(2)}) %collective-permute-start.22) | collective-permute-done | bytes 49184 | tf_op jit(solution)/shard_map/ppermute | solution.py:486
  44.3 3.7 %collective-permute-start.10 = (bf16[4,64,128]{2,1,0:T(8,128)(2,1)S(1)}, bf16[4,64,128]{2,1,0:T(8,128)(2,1)S(1)}, u32[]{:S(2)}, u32[]{:S(2)}) collective-permute-start(bf16[4,64,128]{2,1,0:T(8,128)(2,1)S(1)} %get-tuple-element.52), channel_id=1, source_target_pairs={{0,12},{4,8},{8,4},{12,0},{16,28},{20,24},{24,20},{28,16},{1,13},{... | collective-permute-start | bytes 196616 | tf_op jit(solution)/shard_map/ppermute | solution.py:473
  48.4 1.4 %collective-permute-start.12 = (bf16[4,64,128]{2,1,0:T(8,128)(2,1)S(1)}, bf16[4,64,128]{2,1,0:T(8,128)(2,1)S(1)}, u32[]{:S(2)}, u32[]{:S(2)}) collective-permute-start(bf16[4,64,128]{2,1,0:T(8,128)(2,1)S(1)} %get-tuple-element.54), channel_id=1, source_target_pairs={{0,4},{4,0},{8,12},{12,8},{16,20},{20,16},{24,28},{28,24},{1,5},{5... | collective-permute-start | bytes 196616 | tf_op jit(solution)/shard_map/ppermute | solution.py:473
  49.9 2.5 %collective-permute-start.13 = (bf16[4,64,128]{2,1,0:T(8,128)(2,1)S(1)}, bf16[4,64,128]{2,1,0:T(8,128)(2,1)S(1)}, u32[]{:S(2)}, u32[]{:S(2)}) collective-permute-start(bf16[4,64,128]{2,1,0:T(8,128)(2,1)S(1)} %get-tuple-element.56), channel_id=1, source_target_pairs={{0,28},{4,24},{8,20},{12,16},{16,12},{20,8},{24,4},{28,0},{1,29},{... | collective-permute-start | bytes 196616 | tf_op jit(solution)/shard_map/ppermute | solution.py:473
  53.7 1.4 %collective-permute-start.14 = (bf16[4,64,128]{2,1,0:T(8,128)(2,1)S(1)}, bf16[4,64,128]{2,1,0:T(8,128)(2,1)S(1)}, u32[]{:S(2)}, u32[]{:S(2)}) collective-permute-start(bf16[4,64,128]{2,1,0:T(8,128)(2,1)S(1)} %get-tuple-element.57), channel_id=1, source_target_pairs={{0,24},{4,28},{8,16},{12,20},{16,8},{20,12},{24,0},{28,4},{1,25},{... | collective-permute-start | bytes 196616 | tf_op jit(solution)/shard_map/ppermute | solution.py:473
  55.0 1.1 %collective-permute-start.27 = (bf16[4,64,128]{2,1,0:T(8,128)(2,1)S(1)}, bf16[4,64,128]{2,1,0:T(8,128)(2,1)S(1)}, u32[]{:S(2)}, u32[]{:S(2)}) collective-permute-start(bf16[4,64,128]{2,1,0:T(8,128)(2,1)S(1)} %get-tuple-element.65), channel_id=1, source_target_pairs={{0,16},{4,20},{8,24},{12,28},{16,0},{20,4},{24,8},{28,12},{1,17},{... | collective-permute-start | bytes 196616 | tf_op jit(solution)/shard_map/ppermute | solution.py:473
  56.1 2.7 %collective-permute-start.28 = (bf16[4,64,128]{2,1,0:T(8,128)(2,1)S(1)}, bf16[4,64,128]{2,1,0:T(8,128)(2,1)S(1)}, u32[]{:S(2)}, u32[]{:S(2)}) collective-permute-start(bf16[4,64,128]{2,1,0:T(8,128)(2,1)S(1)} %get-tuple-element.66), channel_id=1, source_target_pairs={{0,20},{4,16},{8,28},{12,24},{16,4},{20,0},{24,12},{28,8},{1,21},{... | collective-permute-start | bytes 196616 | tf_op jit(solution)/shard_map/ppermute | solution.py:473
  59.8 4.7 %collective-permute-done.27.refs_8_.refs_1_ = bf16[4,64,128]{2,1,0:T(8,128)(2,1)S(1)} collective-permute-done((bf16[4,64,128]{2,1,0:T(8,128)(2,1)S(1)}, bf16[4,64,128]{2,1,0:T(8,128)(2,1)S(1)}, u32[]{:S(2)}, u32[]{:S(2)}) %collective-permute-start.27) | collective-permute-done | bytes 65568 | tf_op jit(solution)/shard_map/ppermute | solution.py:473
  64.5 1.6 %collective-permute-done.28.refs_9_.refs_0_ = bf16[4,64,128]{2,1,0:T(8,128)(2,1)S(1)} collective-permute-done((bf16[4,64,128]{2,1,0:T(8,128)(2,1)S(1)}, bf16[4,64,128]{2,1,0:T(8,128)(2,1)S(1)}, u32[]{:S(2)}, u32[]{:S(2)}) %collective-permute-start.28) | collective-permute-done | bytes 65568 | tf_op jit(solution)/shard_map/ppermute | solution.py:473
  66.1 1.1 %down.1 = bf16[8,4,24,128]{3,2,1,0:T(8,128)(2,1)} custom-call(bf16[192,128]{1,0:T(8,128)(2,1)S(1)} %gate_up.1.refs_0_, bf16[192,128]{1,0:T(8,128)(2,1)S(1)} %collective-permute-done.24.refs_1_, bf16[192,128]{1,0:T(8,128)(2,1)S(1)} %collective-permute-done.25.refs_2_, bf16[192,128]{1,0:T(8,128)(2,1)S(1)} %collective-permute-done.26.refs_3_, ...), custom_call_target="tpu_custom_call" | custom-call | tf_op jit(solution)/shard_map/down/pallas_call | solution.py:370
  67.2 2.6 %all-to-all-start = ((bf16[32,24,128]{2,1,0:T(8,128)(2,1)}), bf16[32,24,128]{2,1,0:T(8,128)(2,1)S(1)}, u32[]{:S(2)}, u32[]{:S(2)}) async-start(bf16[32,24,128]{2,1,0:T(8,128)(2,1)} %bitcast.4), calls=%async_computation | async-start | bytes 393216 | tf_op jit(solution)/shard_map/all_to_all | solution.py:533
  70.1 1.6 %collective-permute-start.16 = (bf16[6,64,128]{2,1,0:T(8,128)(2,1)S(1)}, bf16[6,64,128]{2,1,0:T(8,128)(2,1)S(1)}, u32[]{:S(2)}, u32[]{:S(2)}) collective-permute-start(bf16[6,64,128]{2,1,0:T(8,128)(2,1)S(1)} %get-tuple-element.60), channel_id=1, source_target_pairs={{0,2},{1,3},{2,0},{3,1},{4,6},{5,7},{6,4},{7,5},{8,10},{9,11},{10,... | collective-permute-start | bytes 294920 | tf_op jit(solution)/shard_map/ppermute | solution.py:478
  72.4 1.6 %collective-permute-start.30 = (bf16[2,64,128]{2,1,0:T(8,128)(2,1)S(1)}, bf16[2,64,128]{2,1,0:T(8,128)(2,1)S(1)}, u32[]{:S(2)}, u32[]{:S(2)}) collective-permute-start(bf16[2,64,128]{2,1,0:T(8,128)(2,1)S(1)} %get-tuple-element.69), channel_id=1, source_target_pairs={{0,2},{1,3},{2,0},{3,1},{4,6},{5,7},{6,4},{7,5},{8,10},{9,11},{10,... | collective-permute-start | bytes 98312 | tf_op jit(solution)/shard_map/ppermute | solution.py:478
  74.0 3.1 %collective-permute-done.16.refs_10_ = bf16[6,64,128]{2,1,0:T(8,128)(2,1)S(1)} collective-permute-done((bf16[6,64,128]{2,1,0:T(8,128)(2,1)S(1)}, bf16[6,64,128]{2,1,0:T(8,128)(2,1)S(1)}, u32[]{:S(2)}, u32[]{:S(2)}) %collective-permute-start.16) | collective-permute-done | bytes 98336 | tf_op jit(solution)/shard_map/ppermute | solution.py:478
  77.1 1.6 %collective-permute-done.17.refs_11_ = bf16[6,64,128]{2,1,0:T(8,128)(2,1)S(1)} collective-permute-done((bf16[6,64,128]{2,1,0:T(8,128)(2,1)S(1)}, bf16[6,64,128]{2,1,0:T(8,128)(2,1)S(1)}, u32[]{:S(2)}, u32[]{:S(2)}) %collective-permute-start.17) | collective-permute-done | bytes 98336 | tf_op jit(solution)/shard_map/ppermute | solution.py:478
  78.6 1.3 %store.1 = (bf16[1,2048,128]{2,1,0:T(8,128)(2,1)}, bf16[1,2048,128]{2,1,0:T(8,128)(2,1)}, bf16[1,2048,128]{2,1,0:T(8,128)(2,1)}) custom-call(bf16[608,128]{1,0:T(8,128)(2,1)S(1)} %get-tuple-element.40.refs_0_.refs_3_.refs_8_, bf16[608,128]{1,0:T(8,128)(2,1)S(1)} %collective-permute-done.refs_1_.refs_2_.refs_9_, ...), custom_call_target="tpu_custom_call" | custom-call | tf_op jit(solution)/shard_map/store/pallas_call | solution.py:321
  80.1 1.2 %finish.1 = (bf16[64,512]{1,0:T(8,128)(2,1)}, bf16[1,2048,128]{2,1,0:T(8,128)(2,1)}) custom-call(f32[64,6]{1,0:T(8,128)S(1)} %get-tuple-element.64.info_ref, bf16[32,24,128]{2,1,0:T(8,128)(2,1)S(1)} %all-to-all-done.back_ref, bf16[2,64,128]{2,1,0:T(8,128)(2,1)S(1)} %get-tuple-element.67.refs_0_, ...), custom_call_target="tpu_custom_call", output_to_operand_aliasing={{1}: (6, {})} | custom-call | tf_op jit(solution)/shard_map/finish/pallas_call | solution.py:427
  (48 shorter events, 5.7 us)
Async XLA Ops:
  4.3 9.8 %collective-permute-start = (bf16[608,128]{1,0:T(8,128)(2,1)S(1)}, bf16[608,128]{1,0:T(8,128)(2,1)S(1)}, u32[]{:S(2)}, u32[]{:S(2)}) collective-permute-start(bf16[608,128]{1,0:T(8,128)(2,1)S(1)} %get-tuple-element.41), channel_id=1, source_target_pairs={{0,4},{4,0},{8,12},{12,8},{16,20},{20,16},{24,28},{28,24},{1,5},{5... | collective-permute-start | bytes 466952 | tf_op jit(solution)/shard_map/ppermute | solution.py:473
  7.4 7.5 %collective-permute-start.1 = (bf16[608,128]{1,0:T(8,128)(2,1)S(1)}, bf16[608,128]{1,0:T(8,128)(2,1)S(1)}, u32[]{:S(2)}, u32[]{:S(2)}) collective-permute-start(bf16[608,128]{1,0:T(8,128)(2,1)S(1)} %get-tuple-element.42), channel_id=1, source_target_pairs={{0,8},{4,12},{8,0},{12,4},{16,24},{20,28},{24,16},{28,20},{1,9},{5... | collective-permute-start | bytes 466952 | tf_op jit(solution)/shard_map/ppermute | solution.py:473
  8.9 7.9 %collective-permute-start.2 = (bf16[608,128]{1,0:T(8,128)(2,1)S(1)}, bf16[608,128]{1,0:T(8,128)(2,1)S(1)}, u32[]{:S(2)}, u32[]{:S(2)}) collective-permute-start(bf16[608,128]{1,0:T(8,128)(2,1)S(1)} %get-tuple-element.43), channel_id=1, source_target_pairs={{0,12},{4,8},{8,4},{12,0},{16,28},{20,24},{24,20},{28,16},{1,13},{... | collective-permute-start | bytes 466952 | tf_op jit(solution)/shard_map/ppermute | solution.py:473
  8.9 14.1 %collective-permute-start.5 = (bf16[608,128]{1,0:T(8,128)(2,1)S(1)}, bf16[608,128]{1,0:T(8,128)(2,1)S(1)}, u32[]{:S(2)}, u32[]{:S(2)}) collective-permute-start(bf16[608,128]{1,0:T(8,128)(2,1)S(1)} %get-tuple-element.46), channel_id=1, source_target_pairs={{0,24},{4,28},{8,16},{12,20},{16,8},{20,12},{24,0},{28,4},{1,25},{... | collective-permute-start | bytes 466952 | tf_op jit(solution)/shard_map/ppermute | solution.py:473
  12.9 13.3 %collective-permute-start.6 = (bf16[608,128]{1,0:T(8,128)(2,1)S(1)}, bf16[608,128]{1,0:T(8,128)(2,1)S(1)}, u32[]{:S(2)}, u32[]{:S(2)}) collective-permute-start(bf16[608,128]{1,0:T(8,128)(2,1)S(1)} %get-tuple-element.47), channel_id=1, source_target_pairs={{0,28},{4,24},{8,20},{12,16},{16,12},{20,8},{24,4},{28,0},{1,29},{... | collective-permute-start | bytes 466952 | tf_op jit(solution)/shard_map/ppermute | solution.py:473
  14.1 22.9 %collective-permute-start.3 = (bf16[608,128]{1,0:T(8,128)(2,1)S(1)}, bf16[608,128]{1,0:T(8,128)(2,1)S(1)}, u32[]{:S(2)}, u32[]{:S(2)}) collective-permute-start(bf16[608,128]{1,0:T(8,128)(2,1)S(1)} %get-tuple-element.44), channel_id=1, source_target_pairs={{0,16},{4,20},{8,24},{12,28},{16,0},{20,4},{24,8},{28,12},{1,17},{... | collective-permute-start | bytes 466952 | tf_op jit(solution)/shard_map/ppermute | solution.py:473
  14.9 24.7 %collective-permute-start.4 = (bf16[608,128]{1,0:T(8,128)(2,1)S(1)}, bf16[608,128]{1,0:T(8,128)(2,1)S(1)}, u32[]{:S(2)}, u32[]{:S(2)}) collective-permute-start(bf16[608,128]{1,0:T(8,128)(2,1)S(1)} %get-tuple-element.45), channel_id=1, source_target_pairs={{0,20},{4,16},{8,28},{12,24},{16,4},{20,0},{24,12},{28,8},{1,21},{... | collective-permute-start | bytes 466952 | tf_op jit(solution)/shard_map/ppermute | solution.py:473
  26.2 13.3 %collective-permute-start.19 = (bf16[144,512]{1,0:T(8,128)(2,1)S(1)}, bf16[144,512]{1,0:T(8,128)(2,1)S(1)}, u32[]{:S(2)}, u32[]{:S(2)}) collective-permute-start(bf16[144,512]{1,0:T(8,128)(2,1)S(1)} %slot_rows.2.refs_0_), channel_id=1, source_target_pairs={{0,2},{1,3},{2,0},{3,1},{4,6},{5,7},{6,4},{7,5},{8,10},{9,11},{10,... | collective-permute-start | bytes 442376 | tf_op jit(solution)/shard_map/ppermute | solution.py:486
  29.1 10.9 %collective-permute-start.7 = (bf16[8,64,128]{2,1,0:T(8,128)(2,1)S(1)}, bf16[8,64,128]{2,1,0:T(8,128)(2,1)S(1)}, u32[]{:S(2)}, u32[]{:S(2)}) collective-permute-start(bf16[8,64,128]{2,1,0:T(8,128)(2,1)S(1)} %get-tuple-element.49), channel_id=1, source_target_pairs={{0,1},{1,0},{2,3},{3,2},{4,5},{5,4},{6,7},{7,6},{8,9},{9,8},{10,11... | collective-permute-start | bytes 393224 | tf_op jit(solution)/shard_map/ppermute | solution.py:478
  29.2 12.4 %collective-permute-start.8 = (bf16[8,64,128]{2,1,0:T(8,128)(2,1)S(1)}, bf16[8,64,128]{2,1,0:T(8,128)(2,1)S(1)}, u32[]{:S(2)}, u32[]{:S(2)}) collective-permute-start(bf16[8,64,128]{2,1,0:T(8,128)(2,1)S(1)} %get-tuple-element.50), channel_id=1, source_target_pairs={{0,2},{1,3},{2,0},{3,1},{4,6},{5,7},{6,4},{7,5},{8,10},{9,11},{10,... | collective-permute-start | bytes 393224 | tf_op jit(solution)/shard_map/ppermute | solution.py:478
  37.0 7.3 %collective-permute-start.9 = (bf16[8,64,128]{2,1,0:T(8,128)(2,1)S(1)}, bf16[8,64,128]{2,1,0:T(8,128)(2,1)S(1)}, u32[]{:S(2)}, u32[]{:S(2)}) collective-permute-start(bf16[8,64,128]{2,1,0:T(8,128)(2,1)S(1)} %get-tuple-element.51), channel_id=1, source_target_pairs={{0,3},{1,2},{2,1},{3,0},{4,7},{5,6},{6,5},{7,4},{8,11},{9,10},{10,... | collective-permute-start | bytes 393224 | tf_op jit(solution)/shard_map/ppermute | solution.py:478
  39.6 10.3 %collective-permute-start.18 = (bf16[144,512]{1,0:T(8,128)(2,1)S(1)}, bf16[144,512]{1,0:T(8,128)(2,1)S(1)}, u32[]{:S(2)}, u32[]{:S(2)}) collective-permute-start(bf16[144,512]{1,0:T(8,128)(2,1)S(1)} %slot_rows.2.refs_0_), channel_id=1, source_target_pairs={{0,1},{1,0},{2,3},{3,2},{4,5},{5,4},{6,7},{7,6},{8,9},{9,8},{10,11... | collective-permute-start | bytes 442376 | tf_op jit(solution)/shard_map/ppermute | solution.py:486
  39.6 12.8 %collective-permute-start.20 = (bf16[144,512]{1,0:T(8,128)(2,1)S(1)}, bf16[144,512]{1,0:T(8,128)(2,1)S(1)}, u32[]{:S(2)}, u32[]{:S(2)}) collective-permute-start(bf16[144,512]{1,0:T(8,128)(2,1)S(1)} %collective-permute-done.19.refs_2_), channel_id=1, source_target_pairs={{0,1},{1,0},{2,3},{3,2},{4,5},{5,4},{6,7},{7,6},{8,9},{9,8},{10,11... | collective-permute-start | bytes 442376 | tf_op jit(solution)/shard_map/ppermute | solution.py:486
  41.7 6.3 %collective-permute-start.21 = (bf16[48,512]{1,0:T(8,128)(2,1)S(1)}, bf16[48,512]{1,0:T(8,128)(2,1)S(1)}, u32[]{:S(2)}, u32[]{:S(2)}) collective-permute-start(bf16[48,512]{1,0:T(8,128)(2,1)S(1)} %slot_rows.3.refs_4_), channel_id=1, source_target_pairs={{0,1},{1,0},{2,3},{3,2},{4,5},{5,4},{6,7},{7,6},{8,9},{9,8},{10,11... | collective-permute-start | bytes 147464 | tf_op jit(solution)/shard_map/ppermute | solution.py:486
  44.3 4.2 %collective-permute-start.23 = (bf16[48,512]{1,0:T(8,128)(2,1)S(1)}, bf16[48,512]{1,0:T(8,128)(2,1)S(1)}, u32[]{:S(2)}, u32[]{:S(2)}) collective-permute-start(bf16[48,512]{1,0:T(8,128)(2,1)S(1)} %collective-permute-done.22.refs_6_), channel_id=1, source_target_pairs={{0,1},{1,0},{2,3},{3,2},{4,5},{5,4},{6,7},{7,6},{8,9},{9,8},{10,11... | collective-permute-start | bytes 147464 | tf_op jit(solution)/shard_map/ppermute | solution.py:486
  44.3 9.4 %collective-permute-start.10 = (bf16[4,64,128]{2,1,0:T(8,128)(2,1)S(1)}, bf16[4,64,128]{2,1,0:T(8,128)(2,1)S(1)}, u32[]{:S(2)}, u32[]{:S(2)}) collective-permute-start(bf16[4,64,128]{2,1,0:T(8,128)(2,1)S(1)} %get-tuple-element.52), channel_id=1, source_target_pairs={{0,12},{4,8},{8,4},{12,0},{16,28},{20,24},{24,20},{28,16},{1,13},{... | collective-permute-start | bytes 196616 | tf_op jit(solution)/shard_map/ppermute | solution.py:473
  48.0 7.0 %collective-permute-start.11 = (bf16[4,64,128]{2,1,0:T(8,128)(2,1)S(1)}, bf16[4,64,128]{2,1,0:T(8,128)(2,1)S(1)}, u32[]{:S(2)}, u32[]{:S(2)}) collective-permute-start(bf16[4,64,128]{2,1,0:T(8,128)(2,1)S(1)} %get-tuple-element.53), channel_id=1, source_target_pairs={{0,8},{4,12},{8,0},{12,4},{16,24},{20,28},{24,16},{28,20},{1,9},{5... | collective-permute-start | bytes 196616 | tf_op jit(solution)/shard_map/ppermute | solution.py:473
  48.4 7.7 %collective-permute-start.12 = (bf16[4,64,128]{2,1,0:T(8,128)(2,1)S(1)}, bf16[4,64,128]{2,1,0:T(8,128)(2,1)S(1)}, u32[]{:S(2)}, u32[]{:S(2)}) collective-permute-start(bf16[4,64,128]{2,1,0:T(8,128)(2,1)S(1)} %get-tuple-element.54), channel_id=1, source_target_pairs={{0,4},{4,0},{8,12},{12,8},{16,20},{20,16},{24,28},{28,24},{1,5},{5... | collective-permute-start | bytes 196616 | tf_op jit(solution)/shard_map/ppermute | solution.py:473
  49.9 9.0 %collective-permute-start.13 = (bf16[4,64,128]{2,1,0:T(8,128)(2,1)S(1)}, bf16[4,64,128]{2,1,0:T(8,128)(2,1)S(1)}, u32[]{:S(2)}, u32[]{:S(2)}) collective-permute-start(bf16[4,64,128]{2,1,0:T(8,128)(2,1)S(1)} %get-tuple-element.56), channel_id=1, source_target_pairs={{0,28},{4,24},{8,20},{12,16},{16,12},{20,8},{24,4},{28,0},{1,29},{... | collective-permute-start | bytes 196616 | tf_op jit(solution)/shard_map/ppermute | solution.py:473
  53.0 5.9 %collective-permute-start.25 = (bf16[192,128]{1,0:T(8,128)(2,1)S(1)}, bf16[192,128]{1,0:T(8,128)(2,1)S(1)}, u32[]{:S(2)}, u32[]{:S(2)}) collective-permute-start(bf16[192,128]{1,0:T(8,128)(2,1)S(1)} %gate_up.1.refs_0_), channel_id=1, source_target_pairs={{0,2},{1,3},{2,0},{3,1},{4,6},{5,7},{6,4},{7,5},{8,10},{9,11},{10,... | collective-permute-start | bytes 147464 | tf_op jit(solution)/shard_map/ppermute | solution.py:486
  53.7 6.1 %collective-permute-start.14 = (bf16[4,64,128]{2,1,0:T(8,128)(2,1)S(1)}, bf16[4,64,128]{2,1,0:T(8,128)(2,1)S(1)}, u32[]{:S(2)}, u32[]{:S(2)}) collective-permute-start(bf16[4,64,128]{2,1,0:T(8,128)(2,1)S(1)} %get-tuple-element.57), channel_id=1, source_target_pairs={{0,24},{4,28},{8,16},{12,20},{16,8},{20,12},{24,0},{28,4},{1,25},{... | collective-permute-start | bytes 196616 | tf_op jit(solution)/shard_map/ppermute | solution.py:473
  55.0 9.4 %collective-permute-start.27 = (bf16[4,64,128]{2,1,0:T(8,128)(2,1)S(1)}, bf16[4,64,128]{2,1,0:T(8,128)(2,1)S(1)}, u32[]{:S(2)}, u32[]{:S(2)}) collective-permute-start(bf16[4,64,128]{2,1,0:T(8,128)(2,1)S(1)} %get-tuple-element.65), channel_id=1, source_target_pairs={{0,16},{4,20},{8,24},{12,28},{16,0},{20,4},{24,8},{28,12},{1,17},{... | collective-permute-start | bytes 196616 | tf_op jit(solution)/shard_map/ppermute | solution.py:473
  56.1 9.9 %collective-permute-start.28 = (bf16[4,64,128]{2,1,0:T(8,128)(2,1)S(1)}, bf16[4,64,128]{2,1,0:T(8,128)(2,1)S(1)}, u32[]{:S(2)}, u32[]{:S(2)}) collective-permute-start(bf16[4,64,128]{2,1,0:T(8,128)(2,1)S(1)} %get-tuple-element.66), channel_id=1, source_target_pairs={{0,20},{4,16},{8,28},{12,24},{16,4},{20,0},{24,12},{28,8},{1,21},{... | collective-permute-start | bytes 196616 | tf_op jit(solution)/shard_map/ppermute | solution.py:473
  58.9 7.2 %collective-permute-start.24 = (bf16[192,128]{1,0:T(8,128)(2,1)S(1)}, bf16[192,128]{1,0:T(8,128)(2,1)S(1)}, u32[]{:S(2)}, u32[]{:S(2)}) collective-permute-start(bf16[192,128]{1,0:T(8,128)(2,1)S(1)} %gate_up.1.refs_0_), channel_id=1, source_target_pairs={{0,1},{1,0},{2,3},{3,2},{4,5},{5,4},{6,7},{7,6},{8,9},{9,8},{10,11... | collective-permute-start | bytes 147464 | tf_op jit(solution)/shard_map/ppermute | solution.py:486
  58.9 7.2 %collective-permute-start.26 = (bf16[192,128]{1,0:T(8,128)(2,1)S(1)}, bf16[192,128]{1,0:T(8,128)(2,1)S(1)}, u32[]{:S(2)}, u32[]{:S(2)}) collective-permute-start(bf16[192,128]{1,0:T(8,128)(2,1)S(1)} %collective-permute-done.25.refs_2_), channel_id=1, source_target_pairs={{0,1},{1,0},{2,3},{3,2},{4,5},{5,4},{6,7},{7,6},{8,9},{9,8},{10,11... | collective-permute-start | bytes 147464 | tf_op jit(solution)/shard_map/ppermute | solution.py:486
  67.2 13.0 %all-to-all-start = ((bf16[32,24,128]{2,1,0:T(8,128)(2,1)}), bf16[32,24,128]{2,1,0:T(8,128)(2,1)S(1)}, u32[]{:S(2)}, u32[]{:S(2)}) async-start(bf16[32,24,128]{2,1,0:T(8,128)(2,1)} %bitcast.4), calls=%async_computation | async-start | bytes 393216 | tf_op jit(solution)/shard_map/all_to_all | solution.py:533
  69.8 4.2 %collective-permute-start.15 = (bf16[6,64,128]{2,1,0:T(8,128)(2,1)S(1)}, bf16[6,64,128]{2,1,0:T(8,128)(2,1)S(1)}, u32[]{:S(2)}, u32[]{:S(2)}) collective-permute-start(bf16[6,64,128]{2,1,0:T(8,128)(2,1)S(1)} %get-tuple-element.59), channel_id=1, source_target_pairs={{0,1},{1,0},{2,3},{3,2},{4,5},{5,4},{6,7},{7,6},{8,9},{9,8},{10,11... | collective-permute-start | bytes 294920 | tf_op jit(solution)/shard_map/ppermute | solution.py:478
  70.1 6.9 %collective-permute-start.16 = (bf16[6,64,128]{2,1,0:T(8,128)(2,1)S(1)}, bf16[6,64,128]{2,1,0:T(8,128)(2,1)S(1)}, u32[]{:S(2)}, u32[]{:S(2)}) collective-permute-start(bf16[6,64,128]{2,1,0:T(8,128)(2,1)S(1)} %get-tuple-element.60), channel_id=1, source_target_pairs={{0,2},{1,3},{2,0},{3,1},{4,6},{5,7},{6,4},{7,5},{8,10},{9,11},{10,... | collective-permute-start | bytes 294920 | tf_op jit(solution)/shard_map/ppermute | solution.py:478
  71.8 6.9 %collective-permute-start.17 = (bf16[6,64,128]{2,1,0:T(8,128)(2,1)S(1)}, bf16[6,64,128]{2,1,0:T(8,128)(2,1)S(1)}, u32[]{:S(2)}, u32[]{:S(2)}) collective-permute-start(bf16[6,64,128]{2,1,0:T(8,128)(2,1)S(1)} %get-tuple-element.61), channel_id=1, source_target_pairs={{0,3},{1,2},{2,1},{3,0},{4,7},{5,6},{6,5},{7,4},{8,11},{9,10},{10,... | collective-permute-start | bytes 294920 | tf_op jit(solution)/shard_map/ppermute | solution.py:478
  71.8 8.1 %collective-permute-start.29 = (bf16[2,64,128]{2,1,0:T(8,128)(2,1)S(1)}, bf16[2,64,128]{2,1,0:T(8,128)(2,1)S(1)}, u32[]{:S(2)}, u32[]{:S(2)}) collective-permute-start(bf16[2,64,128]{2,1,0:T(8,128)(2,1)S(1)} %get-tuple-element.68), channel_id=1, source_target_pairs={{0,1},{1,0},{2,3},{3,2},{4,5},{5,4},{6,7},{7,6},{8,9},{9,8},{10,11... | collective-permute-start | bytes 98312 | tf_op jit(solution)/shard_map/ppermute | solution.py:478
  72.4 7.8 %collective-permute-start.30 = (bf16[2,64,128]{2,1,0:T(8,128)(2,1)S(1)}, bf16[2,64,128]{2,1,0:T(8,128)(2,1)S(1)}, u32[]{:S(2)}, u32[]{:S(2)}) collective-permute-start(bf16[2,64,128]{2,1,0:T(8,128)(2,1)S(1)} %get-tuple-element.69), channel_id=1, source_target_pairs={{0,2},{1,3},{2,0},{3,1},{4,6},{5,7},{6,4},{7,5},{8,10},{9,11},{10,... | collective-permute-start | bytes 98312 | tf_op jit(solution)/shard_map/ppermute | solution.py:478
  74.0 6.1 %collective-permute-start.31 = (bf16[2,64,128]{2,1,0:T(8,128)(2,1)S(1)}, bf16[2,64,128]{2,1,0:T(8,128)(2,1)S(1)}, u32[]{:S(2)}, u32[]{:S(2)}) collective-permute-start(bf16[2,64,128]{2,1,0:T(8,128)(2,1)S(1)} %get-tuple-element.70), channel_id=1, source_target_pairs={{0,3},{1,2},{2,1},{3,0},{4,7},{5,6},{6,5},{7,4},{8,11},{9,10},{10,... | collective-permute-start | bytes 98312 | tf_op jit(solution)/shard_map/ppermute | solution.py:478
  (2 other events, 4.8 us)

commit v3 on v2

--- a/solution.py
+++ b/solution.py
@@ -135,30 +135,34 @@
     block, cols = weights[0].shape[1:]
     tail = later_rows.shape[1]
 
-    def kernel(rows_ref, gain_ref, *refs):
+    def kernel(rows_ref, gain_in, *refs):
         sources = refs[:stack]
         targets = refs[stack : stack + count]
-        buffer, sems = refs[stack + count :]
+        buffer, gain_ref, sems, gain_sem = refs[stack + count :]
         own, _ = own_places()
         order = [(n, w) for n in range(count) for w in range(stack)]
+        (gain_copy,) = fetch([(gain_in, gain_ref)], gain_sem)
         copies = fetch(
             [(sources[w].at[own ^ steps[n]], buffer.at[n, w]) for n, w in order], sems
         )
-        factor = column(gain_ref[...])
         for n in range(count):
             targets[n][stack * block :, :] = rows_ref[n]
+        gain_copy.wait()
+        factor = column(gain_ref[...])
         for (n, w), copy in zip(order, copies):
             copy.wait()
             targets[n][w * block : (w + 1) * block, :] = (buffer[n, w] * factor).astype(BF16)
 
     return pl.pallas_call(
         kernel,
-        in_specs=[whole(VMEM)] * 2 + [whole(ANY)] * stack,
+        in_specs=[whole(VMEM)] + [whole(ANY)] * (1 + stack),
         out_specs=[whole(VMEM)] * count,
         out_shape=[jax.ShapeDtypeStruct((stack * block + tail, cols), BF16)] * count,
         scratch_shapes=[
             VMEM((count, stack, block, cols), F32),
+            VMEM(gain.shape, F32),
             pltpu.SemaphoreType.DMA((count * stack,)),
+            pltpu.SemaphoreType.DMA((1,)),
         ],
         compiler_params=GRANT,
         name="start_later",
@@ -462,9 +466,8 @@
     capacity = max(2, (3 * tok_rows + experts - 1) // experts)
     block = gate_weight.shape[1]
     far, near = halves_of(n_fs)
-    early = far[: n_fs // 4]
-    later = far[n_fs // 4 :] + near
-    batches = [near + early, far[n_fs // 4 :]]
+    early, later = far[:1], far[1:] + near
+    batches = [near + far[: n_fs // 4], far[n_fs // 4 :]]
     row_order = batches[0] + batches[1]
 
     def swap_fs(value, s):
@@ -509,7 +512,9 @@
         capacity,
         n_fs // n_tp,
     )
-    later_chunks = start_later(later, later_rows, gain, weights)
+    later_chunks = start_later(
+        later, later_rows, pltpu.with_memory_space_constraint(gain, pltpu.HBM), weights
+    )
     local = dict(zip(early + later, list(early_chunks) + list(later_chunks)))
     chunks = [swap_fs(local[s], s) for s in range(n_fs)]
 
@@ -519,15 +524,15 @@
     down_chunks = [swap_fs(down_local[s], s) for s in range(n_fs)]
 
     parts, quarters = [], []
-    for batch in batches:
+    for k, batch in enumerate(batches):
         rows = slot_rows_of([chunks[s] for s in batch], 2 * block, capacity)
-        parts.append(gather_tp(rows))
+        parts.append(gather_tp(rows) if k == 0 else [swap_tp(rows, t) for t in range(n_tp)])
     for batch in batches:
         pieces = regroup([down_chunks[s] for s in batch])
         quarters.append([swap_tp(pieces[t], t) for t in range(n_tp)])
 
     hidden = gate_up(parts, chunks, block)
-    hiddens = gather_tp(hidden)
+    hiddens = [swap_tp(hidden, t) for t in range(n_tp)]
     rows = down(row_order, hiddens, down_chunks, capacity)
     rows = rows.reshape(n_fs * n_tp, *rows.shape[2:])
     back = lax.all_to_all(rows, ("fs", "tp"), split_axis=0, concat_axis=0, tiled=True)

time: 81.9 us -> 76.1 us (0.929)
  waiting for transfers between devices: 33.3 us -> 22.1 us
  starting transfers between devices: 38 us -> 44 us
    ppermute x14, waiting for transfers between devices: 25.8 us -> 16.1 us  [swap_fs(): return lax.ppermute(value, 'fs', [(n, n ^ s) for n in range(n_fs)])]
    ppermute x14, starting transfers between devices: 25.7 us -> 30.6 us  [swap_fs(): return lax.ppermute(value, 'fs', [(n, n ^ s) for n in range(n_fs)])]
    ppermute x9 -> x15, starting transfers between devices: 4.82 us -> 7.65 us  [swap_tp(): return lax.ppermute(value, 'tp', [(n, n ^ s) for n in range(n_tp)])]
    ppermute x9 -> x3, starting transfers between devices: 4.82 us -> 2.07 us  [gather_tp(): lax.ppermute(parts[t], 'tp', [(n, n ^ step) for n in range(n_tp)])]
    ppermute x9 -> x3, waiting for transfers between devices: 2.61 us -> 0.01 us  [gather_tp(): lax.ppermute(parts[t], 'tp', [(n, n ^ step) for n in range(n_tp)])]
    ppermute x9 -> x15, waiting for transfers between devices: 4.84 us -> 6.04 us  [swap_tp(): return lax.ppermute(value, 'tp', [(n, n ^ s) for n in range(n_tp)])]
    all_to_all x1, starting transfers between devices: 2.61 us -> 3.62 us  [exchange_body(): lax.all_to_all(rows, ('fs', 'tp'), split_axis=0, concat_axis=0, tiled=True)]
where the time goes in v3:
time: 76.1 us; the launch traced here: 75.5 us
  starting transfers between devices  44 us (58%)
  waiting for transfers between devices  22.1 us (29%)
  Pallas kernels  8.62 us (11%)
  between operations  0.81 us (1%)
    ppermute x14, starting transfers between devices, swap_fs(): return lax.ppermute(value, 'fs', [(n, n ^ s) for n in range(n_fs)])  30.6 us
    ppermute x14, waiting for transfers between devices, swap_fs(): return lax.ppermute(value, 'fs', [(n, n ^ s) for n in range(n_fs)])  16.1 us
    ppermute x15, starting transfers between devices, swap_tp(): return lax.ppermute(value, 'tp', [(n, n ^ s) for n in range(n_tp)])  7.65 us
    ppermute x15, waiting for transfers between devices, swap_tp(): return lax.ppermute(value, 'tp', [(n, n ^ s) for n in range(n_tp)])  6.04 us
    all_to_all x1, starting transfers between devices, exchange_body(): lax.all_to_all(rows, ('fs', 'tp'), split_axis=0, concat_axis=0, tiled=True)  3.62 us
    ppermute x3, starting transfers between devices, gather_tp(): lax.ppermute(parts[t], 'tp', [(n, n ^ step) for n in range(n_tp)])  2.07 us
    pallas_call x1, Pallas kernels, start_later(): pl.pallas_call(kernel, in_specs=[whole(VMEM)] + [whole(ANY)] * (1 + stack...  1.69 us
  transfers between devices with their start and end apart: 33, of which 11 were waited for; matrix products, arithmetic and copies ran while one was open for 0% of the time, Pallas kernels for 4%

profile of v3, /device:TPU:0, one launch (start us, length us, event | category | flops | bytes accessed | tf_op | source)
XLA Modules:
  0.0 75.5 jit_solution(7345796310772239464)
XLA Ops:
  0.6 1.3 %start_first.1 = (f32[64,6]{1,0:T(8,128)S(1)}, bf16[7,96,128]{2,1,0:T(8,128)(2,1)S(1)}, bf16[608,128]{1,0:T(8,128)(2,1)S(1)}) custom-call(s32[2,64]{1,0:T(2,128)} %bitcast.7, f32[1,64]{1,0:T(1,128)} %bitcast.8, f32[1,64]{1,0:T(1,128)} %bitcast.9, bf16[64,512]{1,0:T(8,128)(2,1)} %refs_3_.1, f32[1,256]{1,0:T(1,128)} %bitcast.5, f32[8,256,128]{2,1,0:T(8,128)} %refs_0_.1, ...), custom_call_target="tpu_custom_call" | custom-call | tf_op jit(solution)/shard_map/start_first/pallas_call | solution.py:113
  1.9 1.7 %start_later.1 = (bf16[608,128]{1,0:T(8,128)(2,1)S(1)}, bf16[608,128]{1,0:T(8,128)(2,1)S(1)}, bf16[608,128]{1,0:T(8,128)(2,1)S(1)}, bf16[608,128]{1,0:T(8,128)(2...) custom-call(bf16[7,96,128]{2,1,0:T(8,128)(2,1)S(1)} %get-tuple-element.39.rows_ref, ...), custom_call_target="tpu_custom_call" | custom-call | tf_op jit(solution)/shard_map/start_later/pallas_call | solution.py:156
  3.6 3.1 %collective-permute-start = (bf16[608,128]{1,0:T(8,128)(2,1)S(1)}, bf16[608,128]{1,0:T(8,128)(2,1)S(1)}, u32[]{:S(2)}, u32[]{:S(2)}) collective-permute-start(bf16[608,128]{1,0:T(8,128)(2,1)S(1)} %get-tuple-element.41), channel_id=1, source_target_pairs={{0,4},{4,0},{8,12},{12,8},{16,20},{20,16},{24,28},{28,24},{1,5},{5... | collective-permute-start | bytes 466952 | tf_op jit(solution)/shard_map/ppermute | solution.py:476
  6.7 1.6 %collective-permute-start.1 = (bf16[608,128]{1,0:T(8,128)(2,1)S(1)}, bf16[608,128]{1,0:T(8,128)(2,1)S(1)}, u32[]{:S(2)}, u32[]{:S(2)}) collective-permute-start(bf16[608,128]{1,0:T(8,128)(2,1)S(1)} %get-tuple-element.42), channel_id=1, source_target_pairs={{0,8},{4,12},{8,0},{12,4},{16,24},{20,28},{24,16},{28,20},{1,9},{5... | collective-permute-start | bytes 466952 | tf_op jit(solution)/shard_map/ppermute | solution.py:476
  8.3 4.0 %collective-permute-start.5 = (bf16[608,128]{1,0:T(8,128)(2,1)S(1)}, bf16[608,128]{1,0:T(8,128)(2,1)S(1)}, u32[]{:S(2)}, u32[]{:S(2)}) collective-permute-start(bf16[608,128]{1,0:T(8,128)(2,1)S(1)} %get-tuple-element.46), channel_id=1, source_target_pairs={{0,24},{4,28},{8,16},{12,20},{16,8},{20,12},{24,0},{28,4},{1,25},{... | collective-permute-start | bytes 466952 | tf_op jit(solution)/shard_map/ppermute | solution.py:476
  12.3 1.2 %collective-permute-start.6 = (bf16[608,128]{1,0:T(8,128)(2,1)S(1)}, bf16[608,128]{1,0:T(8,128)(2,1)S(1)}, u32[]{:S(2)}, u32[]{:S(2)}) collective-permute-start(bf16[608,128]{1,0:T(8,128)(2,1)S(1)} %get-tuple-element.47), channel_id=1, source_target_pairs={{0,28},{4,24},{8,20},{12,16},{16,12},{20,8},{24,4},{28,0},{1,29},{... | collective-permute-start | bytes 466952 | tf_op jit(solution)/shard_map/ppermute | solution.py:476
  13.5 1.4 %cast_rows.1 = (bf16[8,64,128]{2,1,0:T(8,128)(2,1)S(1)}, bf16[8,64,128]{2,1,0:T(8,128)(2,1)S(1)}, bf16[8,64,128]{2,1,0:T(8,128)(2,1)S(1)}, bf16[8,64,128]{2,1,0:T(8,128)(2,1)S(1)}) custom-call(f32[8,256,128]{2,1,0:T(8,128)} %source.1), custom_call_target="tpu_custom_call" | custom-call | tf_op jit(solution)/shard_map/cast_rows/pallas_call | solution.py:211
  14.9 1.3 %collective-permute-start.3 = (bf16[608,128]{1,0:T(8,128)(2,1)S(1)}, bf16[608,128]{1,0:T(8,128)(2,1)S(1)}, u32[]{:S(2)}, u32[]{:S(2)}) collective-permute-start(bf16[608,128]{1,0:T(8,128)(2,1)S(1)} %get-tuple-element.44), channel_id=1, source_target_pairs={{0,16},{4,20},{8,24},{12,28},{16,0},{20,4},{24,8},{28,12},{1,17},{... | collective-permute-start | bytes 466952 | tf_op jit(solution)/shard_map/ppermute | solution.py:476
  16.2 1.5 %collective-permute-start.8 = (bf16[8,64,128]{2,1,0:T(8,128)(2,1)S(1)}, bf16[8,64,128]{2,1,0:T(8,128)(2,1)S(1)}, u32[]{:S(2)}, u32[]{:S(2)}) collective-permute-start(bf16[8,64,128]{2,1,0:T(8,128)(2,1)S(1)} %get-tuple-element.50), channel_id=1, source_target_pairs={{0,2},{1,3},{2,0},{3,1},{4,6},{5,7},{6,4},{7,5},{8,10},{9,11},{10,... | collective-permute-start | bytes 393224 | tf_op jit(solution)/shard_map/ppermute | solution.py:481
  17.7 4.7 %collective-permute-done.5.refs_6_.refs_5_.refs_14_ = bf16[608,128]{1,0:T(8,128)(2,1)S(1)} collective-permute-done((bf16[608,128]{1,0:T(8,128)(2,1)S(1)}, bf16[608,128]{1,0:T(8,128)(2,1)S(1)}, u32[]{:S(2)}, u32[]{:S(2)}) %collective-permute-start.5) | collective-permute-done | bytes 155680 | tf_op jit(solution)/shard_map/ppermute | solution.py:476
  22.4 3.1 %collective-permute-done.6.refs_7_.refs_4_.refs_15_ = bf16[608,128]{1,0:T(8,128)(2,1)S(1)} collective-permute-done((bf16[608,128]{1,0:T(8,128)(2,1)S(1)}, bf16[608,128]{1,0:T(8,128)(2,1)S(1)}, u32[]{:S(2)}, u32[]{:S(2)}) %collective-permute-start.6) | collective-permute-done | bytes 155680 | tf_op jit(solution)/shard_map/ppermute | solution.py:476
  25.6 1.6 %collective-permute-start.19 = (bf16[144,512]{1,0:T(8,128)(2,1)S(1)}, bf16[144,512]{1,0:T(8,128)(2,1)S(1)}, u32[]{:S(2)}, u32[]{:S(2)}) collective-permute-start(bf16[144,512]{1,0:T(8,128)(2,1)S(1)} %slot_rows.2.refs_0_), channel_id=1, source_target_pairs={{0,2},{1,3},{2,0},{3,1},{4,6},{5,7},{6,4},{7,5},{8,10},{9,11},{10,... | collective-permute-start | bytes 442376 | tf_op jit(solution)/shard_map/ppermute | solution.py:489
  27.1 6.3 %collective-permute-start.4 = (bf16[608,128]{1,0:T(8,128)(2,1)S(1)}, bf16[608,128]{1,0:T(8,128)(2,1)S(1)}, u32[]{:S(2)}, u32[]{:S(2)}) collective-permute-start(bf16[608,128]{1,0:T(8,128)(2,1)S(1)} %get-tuple-element.45), channel_id=1, source_target_pairs={{0,20},{4,16},{8,28},{12,24},{16,4},{20,0},{24,12},{28,8},{1,21},{... | collective-permute-start | bytes 466952 | tf_op jit(solution)/shard_map/ppermute | solution.py:476
  33.6 3.5 %collective-permute-start.11 = (bf16[4,64,128]{2,1,0:T(8,128)(2,1)S(1)}, bf16[4,64,128]{2,1,0:T(8,128)(2,1)S(1)}, u32[]{:S(2)}, u32[]{:S(2)}) collective-permute-start(bf16[4,64,128]{2,1,0:T(8,128)(2,1)S(1)} %get-tuple-element.53), channel_id=1, source_target_pairs={{0,8},{4,12},{8,0},{12,4},{16,24},{20,28},{24,16},{28,20},{1,9},{5... | collective-permute-start | bytes 196616 | tf_op jit(solution)/shard_map/ppermute | solution.py:476
  37.8 1.6 %collective-permute-done.10.refs_0_.refs_7_ = bf16[4,64,128]{2,1,0:T(8,128)(2,1)S(1)} collective-permute-done((bf16[4,64,128]{2,1,0:T(8,128)(2,1)S(1)}, bf16[4,64,128]{2,1,0:T(8,128)(2,1)S(1)}, u32[]{:S(2)}, u32[]{:S(2)}) %collective-permute-start.10) | collective-permute-done | bytes 65568 | tf_op jit(solution)/shard_map/ppermute | solution.py:476
  39.4 0.9 %collective-permute-start.22 = (bf16[48,512]{1,0:T(8,128)(2,1)S(1)}, bf16[48,512]{1,0:T(8,128)(2,1)S(1)}, u32[]{:S(2)}, u32[]{:S(2)}) collective-permute-start(bf16[48,512]{1,0:T(8,128)(2,1)S(1)} %slot_rows.3.refs_4_), channel_id=1, source_target_pairs={{0,2},{1,3},{2,0},{3,1},{4,6},{5,7},{6,4},{7,5},{8,10},{9,11},{10,... | collective-permute-start | bytes 147464 | tf_op jit(solution)/shard_map/ppermute | solution.py:481
  40.3 2.0 %collective-permute-start.12 = (bf16[4,64,128]{2,1,0:T(8,128)(2,1)S(1)}, bf16[4,64,128]{2,1,0:T(8,128)(2,1)S(1)}, u32[]{:S(2)}, u32[]{:S(2)}) collective-permute-start(bf16[4,64,128]{2,1,0:T(8,128)(2,1)S(1)} %get-tuple-element.54), channel_id=1, source_target_pairs={{0,4},{4,0},{8,12},{12,8},{16,20},{20,16},{24,28},{28,24},{1,5},{5... | collective-permute-start | bytes 196616 | tf_op jit(solution)/shard_map/ppermute | solution.py:476
  42.4 1.2 %collective-permute-done.22.refs_6_ = bf16[48,512]{1,0:T(8,128)(2,1)S(1)} collective-permute-done((bf16[48,512]{1,0:T(8,128)(2,1)S(1)}, bf16[48,512]{1,0:T(8,128)(2,1)S(1)}, u32[]{:S(2)}, u32[]{:S(2)}) %collective-permute-start.22) | collective-permute-done | bytes 49184 | tf_op jit(solution)/shard_map/ppermute | solution.py:481
  43.6 3.6 %collective-permute-start.13 = (bf16[4,64,128]{2,1,0:T(8,128)(2,1)S(1)}, bf16[4,64,128]{2,1,0:T(8,128)(2,1)S(1)}, u32[]{:S(2)}, u32[]{:S(2)}) collective-permute-start(bf16[4,64,128]{2,1,0:T(8,128)(2,1)S(1)} %get-tuple-element.56), channel_id=1, source_target_pairs={{0,28},{4,24},{8,20},{12,16},{16,12},{20,8},{24,4},{28,0},{1,29},{... | collective-permute-start | bytes 196616 | tf_op jit(solution)/shard_map/ppermute | solution.py:476
  47.2 1.5 %collective-permute-start.14 = (bf16[4,64,128]{2,1,0:T(8,128)(2,1)S(1)}, bf16[4,64,128]{2,1,0:T(8,128)(2,1)S(1)}, u32[]{:S(2)}, u32[]{:S(2)}) collective-permute-start(bf16[4,64,128]{2,1,0:T(8,128)(2,1)S(1)} %get-tuple-element.57), channel_id=1, source_target_pairs={{0,24},{4,28},{8,16},{12,20},{16,8},{20,12},{24,0},{28,4},{1,25},{... | collective-permute-start | bytes 196616 | tf_op jit(solution)/shard_map/ppermute | solution.py:476
  48.7 2.5 %collective-permute-start.28 = (bf16[4,64,128]{2,1,0:T(8,128)(2,1)S(1)}, bf16[4,64,128]{2,1,0:T(8,128)(2,1)S(1)}, u32[]{:S(2)}, u32[]{:S(2)}) collective-permute-start(bf16[4,64,128]{2,1,0:T(8,128)(2,1)S(1)} %get-tuple-element.66), channel_id=1, source_target_pairs={{0,20},{4,16},{8,28},{12,24},{16,4},{20,0},{24,12},{28,8},{1,21},{... | collective-permute-start | bytes 196616 | tf_op jit(solution)/shard_map/ppermute | solution.py:476
  52.8 1.1 %collective-permute-done.14.refs_5_.refs_10_ = bf16[4,64,128]{2,1,0:T(8,128)(2,1)S(1)} collective-permute-done((bf16[4,64,128]{2,1,0:T(8,128)(2,1)S(1)}, bf16[4,64,128]{2,1,0:T(8,128)(2,1)S(1)}, u32[]{:S(2)}, u32[]{:S(2)}) %collective-permute-start.14) | collective-permute-done | bytes 65568 | tf_op jit(solution)/shard_map/ppermute | solution.py:476
  53.9 3.6 %collective-permute-done.27.refs_8_.refs_1_ = bf16[4,64,128]{2,1,0:T(8,128)(2,1)S(1)} collective-permute-done((bf16[4,64,128]{2,1,0:T(8,128)(2,1)S(1)}, bf16[4,64,128]{2,1,0:T(8,128)(2,1)S(1)}, u32[]{:S(2)}, u32[]{:S(2)}) %collective-permute-start.27) | collective-permute-done | bytes 65568 | tf_op jit(solution)/shard_map/ppermute | solution.py:476
  57.5 1.8 %collective-permute-done.28.refs_9_.refs_0_ = bf16[4,64,128]{2,1,0:T(8,128)(2,1)S(1)} collective-permute-done((bf16[4,64,128]{2,1,0:T(8,128)(2,1)S(1)}, bf16[4,64,128]{2,1,0:T(8,128)(2,1)S(1)}, u32[]{:S(2)}, u32[]{:S(2)}) %collective-permute-start.28) | collective-permute-done | bytes 65568 | tf_op jit(solution)/shard_map/ppermute | solution.py:476
  59.3 1.1 %down.1 = bf16[8,4,24,128]{3,2,1,0:T(8,128)(2,1)} custom-call(bf16[192,128]{1,0:T(8,128)(2,1)S(1)} %gate_up.1.refs_0_, bf16[192,128]{1,0:T(8,128)(2,1)S(1)} %collective-permute-done.24.refs_1_, bf16[192,128]{1,0:T(8,128)(2,1)S(1)} %collective-permute-done.25.refs_2_, bf16[192,128]{1,0:T(8,128)(2,1)S(1)} %collective-permute-done.26.refs_3_, ...), custom_call_target="tpu_custom_call" | custom-call | tf_op jit(solution)/shard_map/down/pallas_call | solution.py:374
  60.4 3.6 %all-to-all-start = ((bf16[32,24,128]{2,1,0:T(8,128)(2,1)}), bf16[32,24,128]{2,1,0:T(8,128)(2,1)S(1)}, u32[]{:S(2)}, u32[]{:S(2)}) async-start(bf16[32,24,128]{2,1,0:T(8,128)(2,1)} %bitcast.4), calls=%async_computation | async-start | bytes 393216 | tf_op jit(solution)/shard_map/all_to_all | solution.py:538
  64.4 1.6 %collective-permute-start.16 = (bf16[6,64,128]{2,1,0:T(8,128)(2,1)S(1)}, bf16[6,64,128]{2,1,0:T(8,128)(2,1)S(1)}, u32[]{:S(2)}, u32[]{:S(2)}) collective-permute-start(bf16[6,64,128]{2,1,0:T(8,128)(2,1)S(1)} %get-tuple-element.60), channel_id=1, source_target_pairs={{0,2},{1,3},{2,0},{3,1},{4,6},{5,7},{6,4},{7,5},{8,10},{9,11},{10,... | collective-permute-start | bytes 294920 | tf_op jit(solution)/shard_map/ppermute | solution.py:481
  66.6 1.6 %collective-permute-start.30 = (bf16[2,64,128]{2,1,0:T(8,128)(2,1)S(1)}, bf16[2,64,128]{2,1,0:T(8,128)(2,1)S(1)}, u32[]{:S(2)}, u32[]{:S(2)}) collective-permute-start(bf16[2,64,128]{2,1,0:T(8,128)(2,1)S(1)} %get-tuple-element.69), channel_id=1, source_target_pairs={{0,2},{1,3},{2,0},{3,1},{4,6},{5,7},{6,4},{7,5},{8,10},{9,11},{10,... | collective-permute-start | bytes 98312 | tf_op jit(solution)/shard_map/ppermute | solution.py:481
  68.3 3.1 %collective-permute-done.16.refs_10_ = bf16[6,64,128]{2,1,0:T(8,128)(2,1)S(1)} collective-permute-done((bf16[6,64,128]{2,1,0:T(8,128)(2,1)S(1)}, bf16[6,64,128]{2,1,0:T(8,128)(2,1)S(1)}, u32[]{:S(2)}, u32[]{:S(2)}) %collective-permute-start.16) | collective-permute-done | bytes 98336 | tf_op jit(solution)/shard_map/ppermute | solution.py:481
  71.3 1.5 %collective-permute-done.17.refs_11_ = bf16[6,64,128]{2,1,0:T(8,128)(2,1)S(1)} collective-permute-done((bf16[6,64,128]{2,1,0:T(8,128)(2,1)S(1)}, bf16[6,64,128]{2,1,0:T(8,128)(2,1)S(1)}, u32[]{:S(2)}, u32[]{:S(2)}) %collective-permute-start.17) | collective-permute-done | bytes 98336 | tf_op jit(solution)/shard_map/ppermute | solution.py:481
  72.9 1.3 %store.1 = (bf16[1,2048,128]{2,1,0:T(8,128)(2,1)}, bf16[1,2048,128]{2,1,0:T(8,128)(2,1)}, bf16[1,2048,128]{2,1,0:T(8,128)(2,1)}) custom-call(bf16[608,128]{1,0:T(8,128)(2,1)S(1)} %get-tuple-element.40.refs_0_.refs_3_.refs_8_, bf16[608,128]{1,0:T(8,128)(2,1)S(1)} %collective-permute-done.refs_1_.refs_2_.refs_9_, ...), custom_call_target="tpu_custom_call" | custom-call | tf_op jit(solution)/shard_map/store/pallas_call | solution.py:325
  74.4 1.1 %finish.1 = (bf16[64,512]{1,0:T(8,128)(2,1)}, bf16[1,2048,128]{2,1,0:T(8,128)(2,1)}) custom-call(f32[64,6]{1,0:T(8,128)S(1)} %get-tuple-element.64.info_ref, bf16[32,24,128]{2,1,0:T(8,128)(2,1)S(1)} %all-to-all-done.back_ref, bf16[2,64,128]{2,1,0:T(8,128)(2,1)S(1)} %get-tuple-element.67.refs_0_, ...), custom_call_target="tpu_custom_call", output_to_operand_aliasing={{1}: (6, {})} | custom-call | tf_op jit(solution)/shard_map/finish/pallas_call | solution.py:431
  (46 shorter events, 3.7 us)
Async XLA Ops:
  3.6 11.2 %collective-permute-start = (bf16[608,128]{1,0:T(8,128)(2,1)S(1)}, bf16[608,128]{1,0:T(8,128)(2,1)S(1)}, u32[]{:S(2)}, u32[]{:S(2)}) collective-permute-start(bf16[608,128]{1,0:T(8,128)(2,1)S(1)} %get-tuple-element.41), channel_id=1, source_target_pairs={{0,4},{4,0},{8,12},{12,8},{16,20},{20,16},{24,28},{28,24},{1,5},{5... | collective-permute-start | bytes 466952 | tf_op jit(solution)/shard_map/ppermute | solution.py:476
  6.7 8.2 %collective-permute-start.1 = (bf16[608,128]{1,0:T(8,128)(2,1)S(1)}, bf16[608,128]{1,0:T(8,128)(2,1)S(1)}, u32[]{:S(2)}, u32[]{:S(2)}) collective-permute-start(bf16[608,128]{1,0:T(8,128)(2,1)S(1)} %get-tuple-element.42), channel_id=1, source_target_pairs={{0,8},{4,12},{8,0},{12,4},{16,24},{20,28},{24,16},{28,20},{1,9},{5... | collective-permute-start | bytes 466952 | tf_op jit(solution)/shard_map/ppermute | solution.py:476
  8.3 7.9 %collective-permute-start.2 = (bf16[608,128]{1,0:T(8,128)(2,1)S(1)}, bf16[608,128]{1,0:T(8,128)(2,1)S(1)}, u32[]{:S(2)}, u32[]{:S(2)}) collective-permute-start(bf16[608,128]{1,0:T(8,128)(2,1)S(1)} %get-tuple-element.43), channel_id=1, source_target_pairs={{0,12},{4,8},{8,4},{12,0},{16,28},{20,24},{24,20},{28,16},{1,13},{... | collective-permute-start | bytes 466952 | tf_op jit(solution)/shard_map/ppermute | solution.py:476
  8.3 14.1 %collective-permute-start.5 = (bf16[608,128]{1,0:T(8,128)(2,1)S(1)}, bf16[608,128]{1,0:T(8,128)(2,1)S(1)}, u32[]{:S(2)}, u32[]{:S(2)}) collective-permute-start(bf16[608,128]{1,0:T(8,128)(2,1)S(1)} %get-tuple-element.46), channel_id=1, source_target_pairs={{0,24},{4,28},{8,16},{12,20},{16,8},{20,12},{24,0},{28,4},{1,25},{... | collective-permute-start | bytes 466952 | tf_op jit(solution)/shard_map/ppermute | solution.py:476
  12.3 13.3 %collective-permute-start.6 = (bf16[608,128]{1,0:T(8,128)(2,1)S(1)}, bf16[608,128]{1,0:T(8,128)(2,1)S(1)}, u32[]{:S(2)}, u32[]{:S(2)}) collective-permute-start(bf16[608,128]{1,0:T(8,128)(2,1)S(1)} %get-tuple-element.47), channel_id=1, source_target_pairs={{0,28},{4,24},{8,20},{12,16},{16,12},{20,8},{24,4},{28,0},{1,29},{... | collective-permute-start | bytes 466952 | tf_op jit(solution)/shard_map/ppermute | solution.py:476
  14.8 12.3 %collective-permute-start.7 = (bf16[8,64,128]{2,1,0:T(8,128)(2,1)S(1)}, bf16[8,64,128]{2,1,0:T(8,128)(2,1)S(1)}, u32[]{:S(2)}, u32[]{:S(2)}) collective-permute-start(bf16[8,64,128]{2,1,0:T(8,128)(2,1)S(1)} %get-tuple-element.49), channel_id=1, source_target_pairs={{0,1},{1,0},{2,3},{3,2},{4,5},{5,4},{6,7},{7,6},{8,9},{9,8},{10,11... | collective-permute-start | bytes 393224 | tf_op jit(solution)/shard_map/ppermute | solution.py:481
  14.9 22.2 %collective-permute-start.3 = (bf16[608,128]{1,0:T(8,128)(2,1)S(1)}, bf16[608,128]{1,0:T(8,128)(2,1)S(1)}, u32[]{:S(2)}, u32[]{:S(2)}) collective-permute-start(bf16[608,128]{1,0:T(8,128)(2,1)S(1)} %get-tuple-element.44), channel_id=1, source_target_pairs={{0,16},{4,20},{8,24},{12,28},{16,0},{20,4},{24,8},{28,12},{1,17},{... | collective-permute-start | bytes 466952 | tf_op jit(solution)/shard_map/ppermute | solution.py:476
  16.2 17.3 %collective-permute-start.8 = (bf16[8,64,128]{2,1,0:T(8,128)(2,1)S(1)}, bf16[8,64,128]{2,1,0:T(8,128)(2,1)S(1)}, u32[]{:S(2)}, u32[]{:S(2)}) collective-permute-start(bf16[8,64,128]{2,1,0:T(8,128)(2,1)S(1)} %get-tuple-element.50), channel_id=1, source_target_pairs={{0,2},{1,3},{2,0},{3,1},{4,6},{5,7},{6,4},{7,5},{8,10},{9,11},{10,... | collective-permute-start | bytes 393224 | tf_op jit(solution)/shard_map/ppermute | solution.py:481
  22.4 11.1 %collective-permute-start.9 = (bf16[8,64,128]{2,1,0:T(8,128)(2,1)S(1)}, bf16[8,64,128]{2,1,0:T(8,128)(2,1)S(1)}, u32[]{:S(2)}, u32[]{:S(2)}) collective-permute-start(bf16[8,64,128]{2,1,0:T(8,128)(2,1)S(1)} %get-tuple-element.51), channel_id=1, source_target_pairs={{0,3},{1,2},{2,1},{3,0},{4,7},{5,6},{6,5},{7,4},{8,11},{9,10},{10,... | collective-permute-start | bytes 393224 | tf_op jit(solution)/shard_map/ppermute | solution.py:481
  25.6 11.5 %collective-permute-start.19 = (bf16[144,512]{1,0:T(8,128)(2,1)S(1)}, bf16[144,512]{1,0:T(8,128)(2,1)S(1)}, u32[]{:S(2)}, u32[]{:S(2)}) collective-permute-start(bf16[144,512]{1,0:T(8,128)(2,1)S(1)} %slot_rows.2.refs_0_), channel_id=1, source_target_pairs={{0,2},{1,3},{2,0},{3,1},{4,6},{5,7},{6,4},{7,5},{8,10},{9,11},{10,... | collective-permute-start | bytes 442376 | tf_op jit(solution)/shard_map/ppermute | solution.py:489
  27.1 10.5 %collective-permute-start.4 = (bf16[608,128]{1,0:T(8,128)(2,1)S(1)}, bf16[608,128]{1,0:T(8,128)(2,1)S(1)}, u32[]{:S(2)}, u32[]{:S(2)}) collective-permute-start(bf16[608,128]{1,0:T(8,128)(2,1)S(1)} %get-tuple-element.45), channel_id=1, source_target_pairs={{0,20},{4,16},{8,28},{12,24},{16,4},{20,0},{24,12},{28,8},{1,21},{... | collective-permute-start | bytes 466952 | tf_op jit(solution)/shard_map/ppermute | solution.py:476
  33.5 5.9 %collective-permute-start.10 = (bf16[4,64,128]{2,1,0:T(8,128)(2,1)S(1)}, bf16[4,64,128]{2,1,0:T(8,128)(2,1)S(1)}, u32[]{:S(2)}, u32[]{:S(2)}) collective-permute-start(bf16[4,64,128]{2,1,0:T(8,128)(2,1)S(1)} %get-tuple-element.52), channel_id=1, source_target_pairs={{0,12},{4,8},{8,4},{12,0},{16,28},{20,24},{24,20},{28,16},{1,13},{... | collective-permute-start | bytes 196616 | tf_op jit(solution)/shard_map/ppermute | solution.py:476
  33.6 6.8 %collective-permute-start.11 = (bf16[4,64,128]{2,1,0:T(8,128)(2,1)S(1)}, bf16[4,64,128]{2,1,0:T(8,128)(2,1)S(1)}, u32[]{:S(2)}, u32[]{:S(2)}) collective-permute-start(bf16[4,64,128]{2,1,0:T(8,128)(2,1)S(1)} %get-tuple-element.53), channel_id=1, source_target_pairs={{0,8},{4,12},{8,0},{12,4},{16,24},{20,28},{24,16},{28,20},{1,9},{5... | collective-permute-start | bytes 196616 | tf_op jit(solution)/shard_map/ppermute | solution.py:476
  37.1 11.6 %collective-permute-start.18 = (bf16[144,512]{1,0:T(8,128)(2,1)S(1)}, bf16[144,512]{1,0:T(8,128)(2,1)S(1)}, u32[]{:S(2)}, u32[]{:S(2)}) collective-permute-start(bf16[144,512]{1,0:T(8,128)(2,1)S(1)} %slot_rows.2.refs_0_), channel_id=1, source_target_pairs={{0,1},{1,0},{2,3},{3,2},{4,5},{5,4},{6,7},{7,6},{8,9},{9,8},{10,11... | collective-permute-start | bytes 442376 | tf_op jit(solution)/shard_map/ppermute | solution.py:489
  37.1 11.6 %collective-permute-start.20 = (bf16[144,512]{1,0:T(8,128)(2,1)S(1)}, bf16[144,512]{1,0:T(8,128)(2,1)S(1)}, u32[]{:S(2)}, u32[]{:S(2)}) collective-permute-start(bf16[144,512]{1,0:T(8,128)(2,1)S(1)} %collective-permute-done.19.refs_2_), channel_id=1, source_target_pairs={{0,1},{1,0},{2,3},{3,2},{4,5},{5,4},{6,7},{7,6},{8,9},{9,8},{10,11... | collective-permute-start | bytes 442376 | tf_op jit(solution)/shard_map/ppermute | solution.py:489
  39.4 4.2 %collective-permute-start.22 = (bf16[48,512]{1,0:T(8,128)(2,1)S(1)}, bf16[48,512]{1,0:T(8,128)(2,1)S(1)}, u32[]{:S(2)}, u32[]{:S(2)}) collective-permute-start(bf16[48,512]{1,0:T(8,128)(2,1)S(1)} %slot_rows.3.refs_4_), channel_id=1, source_target_pairs={{0,2},{1,3},{2,0},{3,1},{4,6},{5,7},{6,4},{7,5},{8,10},{9,11},{10,... | collective-permute-start | bytes 147464 | tf_op jit(solution)/shard_map/ppermute | solution.py:481
  40.3 6.8 %collective-permute-start.23 = (bf16[48,512]{1,0:T(8,128)(2,1)S(1)}, bf16[48,512]{1,0:T(8,128)(2,1)S(1)}, u32[]{:S(2)}, u32[]{:S(2)}) collective-permute-start(bf16[48,512]{1,0:T(8,128)(2,1)S(1)} %slot_rows.3.refs_4_), channel_id=1, source_target_pairs={{0,3},{1,2},{2,1},{3,0},{4,7},{5,6},{6,5},{7,4},{8,11},{9,10},{10,... | collective-permute-start | bytes 147464 | tf_op jit(solution)/shard_map/ppermute | solution.py:481
  40.3 11.5 %collective-permute-start.12 = (bf16[4,64,128]{2,1,0:T(8,128)(2,1)S(1)}, bf16[4,64,128]{2,1,0:T(8,128)(2,1)S(1)}, u32[]{:S(2)}, u32[]{:S(2)}) collective-permute-start(bf16[4,64,128]{2,1,0:T(8,128)(2,1)S(1)} %get-tuple-element.54), channel_id=1, source_target_pairs={{0,4},{4,0},{8,12},{12,8},{16,20},{20,16},{24,28},{28,24},{1,5},{5... | collective-permute-start | bytes 196616 | tf_op jit(solution)/shard_map/ppermute | solution.py:476
  43.6 8.4 %collective-permute-start.13 = (bf16[4,64,128]{2,1,0:T(8,128)(2,1)S(1)}, bf16[4,64,128]{2,1,0:T(8,128)(2,1)S(1)}, u32[]{:S(2)}, u32[]{:S(2)}) collective-permute-start(bf16[4,64,128]{2,1,0:T(8,128)(2,1)S(1)} %get-tuple-element.56), channel_id=1, source_target_pairs={{0,28},{4,24},{8,20},{12,16},{16,12},{20,8},{24,4},{28,0},{1,29},{... | collective-permute-start | bytes 196616 | tf_op jit(solution)/shard_map/ppermute | solution.py:476
  47.2 6.7 %collective-permute-start.14 = (bf16[4,64,128]{2,1,0:T(8,128)(2,1)S(1)}, bf16[4,64,128]{2,1,0:T(8,128)(2,1)S(1)}, u32[]{:S(2)}, u32[]{:S(2)}) collective-permute-start(bf16[4,64,128]{2,1,0:T(8,128)(2,1)S(1)} %get-tuple-element.57), channel_id=1, source_target_pairs={{0,24},{4,28},{8,16},{12,20},{16,8},{20,12},{24,0},{28,4},{1,25},{... | collective-permute-start | bytes 196616 | tf_op jit(solution)/shard_map/ppermute | solution.py:476
  48.7 8.8 %collective-permute-start.27 = (bf16[4,64,128]{2,1,0:T(8,128)(2,1)S(1)}, bf16[4,64,128]{2,1,0:T(8,128)(2,1)S(1)}, u32[]{:S(2)}, u32[]{:S(2)}) collective-permute-start(bf16[4,64,128]{2,1,0:T(8,128)(2,1)S(1)} %get-tuple-element.65), channel_id=1, source_target_pairs={{0,16},{4,20},{8,24},{12,28},{16,0},{20,4},{24,8},{28,12},{1,17},{... | collective-permute-start | bytes 196616 | tf_op jit(solution)/shard_map/ppermute | solution.py:476
  48.7 10.6 %collective-permute-start.28 = (bf16[4,64,128]{2,1,0:T(8,128)(2,1)S(1)}, bf16[4,64,128]{2,1,0:T(8,128)(2,1)S(1)}, u32[]{:S(2)}, u32[]{:S(2)}) collective-permute-start(bf16[4,64,128]{2,1,0:T(8,128)(2,1)S(1)} %get-tuple-element.66), channel_id=1, source_target_pairs={{0,20},{4,16},{8,28},{12,24},{16,4},{20,0},{24,12},{28,8},{1,21},{... | collective-permute-start | bytes 196616 | tf_op jit(solution)/shard_map/ppermute | solution.py:476
  51.9 7.4 %collective-permute-start.24 = (bf16[192,128]{1,0:T(8,128)(2,1)S(1)}, bf16[192,128]{1,0:T(8,128)(2,1)S(1)}, u32[]{:S(2)}, u32[]{:S(2)}) collective-permute-start(bf16[192,128]{1,0:T(8,128)(2,1)S(1)} %gate_up.1.refs_0_), channel_id=1, source_target_pairs={{0,1},{1,0},{2,3},{3,2},{4,5},{5,4},{6,7},{7,6},{8,9},{9,8},{10,11... | collective-permute-start | bytes 147464 | tf_op jit(solution)/shard_map/ppermute | solution.py:481
  52.0 7.4 %collective-permute-start.25 = (bf16[192,128]{1,0:T(8,128)(2,1)S(1)}, bf16[192,128]{1,0:T(8,128)(2,1)S(1)}, u32[]{:S(2)}, u32[]{:S(2)}) collective-permute-start(bf16[192,128]{1,0:T(8,128)(2,1)S(1)} %gate_up.1.refs_0_), channel_id=1, source_target_pairs={{0,2},{1,3},{2,0},{3,1},{4,6},{5,7},{6,4},{7,5},{8,10},{9,11},{10,... | collective-permute-start | bytes 147464 | tf_op jit(solution)/shard_map/ppermute | solution.py:481
  53.9 5.5 %collective-permute-start.26 = (bf16[192,128]{1,0:T(8,128)(2,1)S(1)}, bf16[192,128]{1,0:T(8,128)(2,1)S(1)}, u32[]{:S(2)}, u32[]{:S(2)}) collective-permute-start(bf16[192,128]{1,0:T(8,128)(2,1)S(1)} %gate_up.1.refs_0_), channel_id=1, source_target_pairs={{0,3},{1,2},{2,1},{3,0},{4,7},{5,6},{6,5},{7,4},{8,11},{9,10},{10,... | collective-permute-start | bytes 147464 | tf_op jit(solution)/shard_map/ppermute | solution.py:481
  60.4 14.0 %all-to-all-start = ((bf16[32,24,128]{2,1,0:T(8,128)(2,1)}), bf16[32,24,128]{2,1,0:T(8,128)(2,1)S(1)}, u32[]{:S(2)}, u32[]{:S(2)}) async-start(bf16[32,24,128]{2,1,0:T(8,128)(2,1)} %bitcast.4), calls=%async_computation | async-start | bytes 393216 | tf_op jit(solution)/shard_map/all_to_all | solution.py:538
  64.1 4.2 %collective-permute-start.15 = (bf16[6,64,128]{2,1,0:T(8,128)(2,1)S(1)}, bf16[6,64,128]{2,1,0:T(8,128)(2,1)S(1)}, u32[]{:S(2)}, u32[]{:S(2)}) collective-permute-start(bf16[6,64,128]{2,1,0:T(8,128)(2,1)S(1)} %get-tuple-element.59), channel_id=1, source_target_pairs={{0,1},{1,0},{2,3},{3,2},{4,5},{5,4},{6,7},{7,6},{8,9},{9,8},{10,11... | collective-permute-start | bytes 294920 | tf_op jit(solution)/shard_map/ppermute | solution.py:481
  64.4 6.9 %collective-permute-start.16 = (bf16[6,64,128]{2,1,0:T(8,128)(2,1)S(1)}, bf16[6,64,128]{2,1,0:T(8,128)(2,1)S(1)}, u32[]{:S(2)}, u32[]{:S(2)}) collective-permute-start(bf16[6,64,128]{2,1,0:T(8,128)(2,1)S(1)} %get-tuple-element.60), channel_id=1, source_target_pairs={{0,2},{1,3},{2,0},{3,1},{4,6},{5,7},{6,4},{7,5},{8,10},{9,11},{10,... | collective-permute-start | bytes 294920 | tf_op jit(solution)/shard_map/ppermute | solution.py:481
  66.0 6.9 %collective-permute-start.17 = (bf16[6,64,128]{2,1,0:T(8,128)(2,1)S(1)}, bf16[6,64,128]{2,1,0:T(8,128)(2,1)S(1)}, u32[]{:S(2)}, u32[]{:S(2)}) collective-permute-start(bf16[6,64,128]{2,1,0:T(8,128)(2,1)S(1)} %get-tuple-element.61), channel_id=1, source_target_pairs={{0,3},{1,2},{2,1},{3,0},{4,7},{5,6},{6,5},{7,4},{8,11},{9,10},{10,... | collective-permute-start | bytes 294920 | tf_op jit(solution)/shard_map/ppermute | solution.py:481
  66.1 8.1 %collective-permute-start.29 = (bf16[2,64,128]{2,1,0:T(8,128)(2,1)S(1)}, bf16[2,64,128]{2,1,0:T(8,128)(2,1)S(1)}, u32[]{:S(2)}, u32[]{:S(2)}) collective-permute-start(bf16[2,64,128]{2,1,0:T(8,128)(2,1)S(1)} %get-tuple-element.68), channel_id=1, source_target_pairs={{0,1},{1,0},{2,3},{3,2},{4,5},{5,4},{6,7},{7,6},{8,9},{9,8},{10,11... | collective-permute-start | bytes 98312 | tf_op jit(solution)/shard_map/ppermute | solution.py:481
  66.6 7.8 %collective-permute-start.30 = (bf16[2,64,128]{2,1,0:T(8,128)(2,1)S(1)}, bf16[2,64,128]{2,1,0:T(8,128)(2,1)S(1)}, u32[]{:S(2)}, u32[]{:S(2)}) collective-permute-start(bf16[2,64,128]{2,1,0:T(8,128)(2,1)S(1)} %get-tuple-element.69), channel_id=1, source_target_pairs={{0,2},{1,3},{2,0},{3,1},{4,6},{5,7},{6,4},{7,5},{8,10},{9,11},{10,... | collective-permute-start | bytes 98312 | tf_op jit(solution)/shard_map/ppermute | solution.py:481
  68.3 6.1 %collective-permute-start.31 = (bf16[2,64,128]{2,1,0:T(8,128)(2,1)S(1)}, bf16[2,64,128]{2,1,0:T(8,128)(2,1)S(1)}, u32[]{:S(2)}, u32[]{:S(2)}) collective-permute-start(bf16[2,64,128]{2,1,0:T(8,128)(2,1)S(1)} %get-tuple-element.70), channel_id=1, source_target_pairs={{0,3},{1,2},{2,1},{3,0},{4,7},{5,6},{6,5},{7,4},{8,11},{9,10},{10,... | collective-permute-start | bytes 98312 | tf_op jit(solution)/shard_map/ppermute | solution.py:481
  (1 other events, 2.7 us)
